TPU v7x, 32 devices: a whole 2x2x4 slice. The times are simulated.
32 devices in a mesh: sp: 8 (over z, y), tp: 4 (over x, core).
Axes of the slice: x: 2, y: 2, z: 4, core: 2. Of those that a mesh axis runs over, the one named last changes fastest.
Arguments:
- queries: bfloat16 [4096, 1024], P('sp', 'tp'), may hold values from -6 to 6
- key_heads: bfloat16 [4096, 512], P('sp', 'tp'), may hold values from -6 to 6
- value_heads: bfloat16 [4096, 512], P('sp', 'tp'), may hold values from -70 to 70
- documents: int32 [4096], P('sp'), may hold values from 0 to 2, never falling along the last dimension, each value on 1 to 2560 neighbouring positions
- query_gain: float32 [128], replicated, may hold values from 0.1 to 8
- key_gain: float32 [128], replicated, may hold values from 0.1 to 8
- out_gain: float32 [1024], replicated, may hold values from 0.1 to 1.9
- out_proj: bfloat16 [1024, 2048], replicated, may hold values from -0.1875 to 0.1875
- residual: bfloat16 [4096, 2048], P(('sp', 'tp')), may hold values from -6 to 6
- mid_gain: float32 [2048], replicated, may hold values from 0.1 to 1.9
- mid_bias: float32 [2048], replicated, may hold values from -1.5 to 1.5
- routes: int32 [4096, 2], P(('sp', 'tp')), may hold values from 0 to 31, all different within a row; in each aligned block of 128 rows (0 to 127, 128 to 255, ...) at most 16 rows name the same one
- route_weights: float32 [4096, 2], P(('sp', 'tp')), may hold values from 0.2 to 2
- expert_gate: bfloat16 [32, 2048, 512], P(('sp', 'tp')), may hold values from -0.125 to 0.125
- expert_up: bfloat16 [32, 2048, 512], P(('sp', 'tp')), may hold values from -0.125 to 0.125
- expert_down: bfloat16 [32, 512, 2048], P(('sp', 'tp')), may hold values from -0.25 to 0.25
- final_gain: float32 [2048], replicated, may hold values from 0.1 to 1.9
- final_bias: float32 [2048], replicated, may hold values from -1.5 to 1.5
Outputs:
- layer_out: bfloat16 [4096, 2048], P(('sp', 'tp'))
Inputs may be any that keep to these rules, and one draw needn't show every extreme that they name: `documents`: never falls along the sequence; each document holds 1 to 2560 positions and one holds exactly 2560. `routes`: each row names 2 different experts; among the rows of one device (aligned blocks of 128 rows) no expert is named more than 16 times, and exactly 16 times in some block.
All inputs are finite; a program needn't handle non-finite values.
Results may differ from a plain program's by a relative error of at most 0.014.
The roundings to bfloat16 on the way count: a program that leaves them out, or rounds other values in their place, can miss the bound.
Values may be sent and summed in bfloat16 or wider, within the bound.
A program may use at most 128 MiB of HBM per device.

v0:
```python
import functools

import jax
import jax.numpy as jnp
from jax import lax
from jax.experimental import pallas as pl
from jax.experimental.pallas import tpu as pltpu
from jax.sharding import PartitionSpec as P

HEAD = 128
GRID = 64


eps_norm = 1e-06
alpha_mix = 8.0**0.25
theta_base = 10000.0
score_factor = HEAD ** (-0.5) * 1.4426950408889634
VMEM = pl.BlockSpec(memory_space=pltpu.VMEM)
ANY = pl.BlockSpec(memory_space=pl.ANY)
SMEM = pl.BlockSpec(memory_space=pltpu.SMEM)


def rotary_tables(row_total, offset):
    positions = offset + jnp.arange(row_total, dtype=jnp.int32)
    grid_row = (positions // GRID).astype(jnp.float32)
    grid_col = (positions % GRID).astype(jnp.float32)
    pair_count = HEAD // 4
    inv_freq = theta_base ** (-jnp.arange(pair_count, dtype=jnp.float32) / pair_count)
    angles = jnp.concatenate(
        [grid_row[:, None] * inv_freq[None, :], grid_col[:, None] * inv_freq[None, :]], axis=1
    )
    return (jnp.cos(angles), jnp.sin(angles))


def normed_rotated(heads_in, gain_vec, cosine_table, sine_table):
    values = heads_in.astype(jnp.float32)
    inv_rms = lax.rsqrt(jnp.mean(values * values, axis=-1, keepdims=True) + eps_norm)
    values = values * inv_rms * gain_vec
    half_dim = HEAD // 2
    first_half = values[..., :half_dim]
    second_half = values[..., half_dim:]
    cosine_part = cosine_table[:, None, :]
    sine_part = sine_table[:, None, :]
    turned = jnp.concatenate(
        [
            first_half * cosine_part - second_half * sine_part,
            second_half * cosine_part + first_half * sine_part,
        ],
        axis=-1,
    )
    return turned.astype(jnp.bfloat16)


def layer_norm(stream, gain_vec, bias_vec):
    center = jnp.mean(stream, axis=-1, keepdims=True)
    spread = jnp.mean(jnp.square(stream - center), axis=-1, keepdims=True)
    return (stream - center) * lax.rsqrt(spread + eps_norm) * gain_vec + bias_vec


def barrier_with(peers):
    barrier = pltpu.get_barrier_semaphore()
    for peer in peers:
        pl.semaphore_signal(barrier, inc=1, device_id=peer, device_id_type=pl.DeviceIdType.MESH)
    pl.semaphore_wait(barrier, len(peers))


def flipped(number, pattern):
    bit = 1
    while bit <= pattern:
        if pattern & bit:
            number = number + bit - 2 * bit * lax.rem(number // bit, 2)
        bit *= 2
    return number


def gather_kernel(
    size,
    pair,
    capacity,
    kv_ref,
    doc_ref,
    q_ref,
    q_gain_ref,
    cos_ref,
    sin_ref,
    route_ref,
    kv_all,
    doc_all,
    q_out,
    column_out,
    row_out,
    kv_send,
    kv_recv,
    doc_send,
    doc_recv,
    own_sem,
):
    me = lax.axis_index("sp")
    inner = lax.rem(me, pair)
    outer = me // pair
    outer_size = size // pair
    parts = kv_ref.shape[0]
    paired = outer_size & (outer_size - 1) == 0
    half = outer_size // 2
    upper, lower = list(range(half, outer_size)), list(range(1, half))
    send_order = [group for group in upper + lower if group]
    work_order = [group for group in upper[:1] + lower + upper[1:] if group]
    own = [
        pltpu.make_async_copy(kv_ref, kv_all.at[me], own_sem.at[0]),
        pltpu.make_async_copy(doc_ref, doc_all.at[me], own_sem.at[1]),
    ]
    for copy in own:
        copy.start()

    def plane(group, sign):
        if paired:
            return flipped(outer, group)
        return lax.rem(outer + sign * group + outer_size, outer_size)

    mate = outer * pair + lax.rem(inner + 1, pair)
    peers = [{"sp": plane(group, 1) * pair + inner} for group in send_order]
    if pair == 2:
        peers.append({"sp": mate})
    barrier_with(peers)

    def send(from_kv, from_doc, place, slot, target):
        copies = [
            pltpu.make_async_remote_copy(
                src_ref=from_kv.at[part],
                dst_ref=kv_all.at[place, part],
                send_sem=kv_send.at[slot, part],
                recv_sem=kv_recv.at[slot, part],
                device_id={"sp": target},
                device_id_type=pl.DeviceIdType.MESH,
            )
            for part in range(parts)
        ]
        copies.append(
            pltpu.make_async_remote_copy(
                src_ref=from_doc,
                dst_ref=doc_all.at[place],
                send_sem=doc_send.at[slot],
                recv_sem=doc_recv.at[slot],
                device_id={"sp": target},
                device_id_type=pl.DeviceIdType.MESH,
            )
        )
        return copies

    sent = []
    far_copies = {}
    for group in send_order:
        copies = send(kv_ref, doc_ref, me, group - 1, plane(group, 1) * pair + inner)
        far_copies[group] = copies
        for copy in copies:
            copy.start()
        sent += copies
    mate_copies = []
    if pair == 2:
        mate_copies += send(kv_ref, doc_ref, me, outer_size - 1, mate)
        for copy in mate_copies:
            copy.start()

    rows, width = q_out.shape[1], q_out.shape[2]
    cosine = jnp.concatenate([cos_ref[...], cos_ref[...]], axis=1)
    sine = jnp.concatenate([-sin_ref[...], sin_ref[...]], axis=1)
    for head in range(q_out.shape[0]):
        values = q_ref[:, head * width : (head + 1) * width].astype(jnp.float32)
        inv_rms = lax.rsqrt(jnp.mean(values * values, axis=1, keepdims=True) + eps_norm)
        values = values * inv_rms * q_gain_ref[...]
        crossed = jnp.concatenate([values[:, width // 2 :], values[:, : width // 2]], axis=1)
        q_out[head] = (values * cosine + crossed * sine).astype(jnp.bfloat16)

    tokens, top = column_out.shape
    experts = 2 * tokens * top // capacity
    down = lax.broadcasted_iota(jnp.int32, (tokens, tokens), 0)
    across = lax.broadcasted_iota(jnp.int32, (tokens, tokens), 1)
    earlier = jnp.where(down > across, 1.0, 0.0).astype(jnp.bfloat16)
    names = lax.broadcasted_iota(jnp.int32, (tokens, experts), 1)
    passed = jnp.zeros((1, experts), jnp.float32)
    for route in range(top):
        named = route_ref[:, route : route + 1]
        one_hot = jnp.where(names == named, 1.0, 0.0)
        before = passed + jnp.dot(
            earlier, one_hot.astype(jnp.bfloat16), preferred_element_type=jnp.float32
        )
        rank = jnp.sum(before * one_hot, axis=1, keepdims=True)
        slot = named.astype(jnp.float32) * capacity + rank
        column_out[:, route : route + 1] = slot.astype(jnp.int32)
        row = jnp.sum(jnp.where(down == across, slot, 0.0), axis=0, keepdims=True)
        row_out[route : route + 1, :] = row.astype(jnp.int32)
        passed = passed + jnp.sum(one_hot, axis=0, keepdims=True)

    for group in work_order:
        place = plane(group, -1) * pair + inner
        forward = []
        if pair == 2:
            forward = send(kv_all.at[place], doc_all.at[place], place, outer_size - 1 + group, mate)
        for number, copy in enumerate(far_copies[group]):
            copy.wait_recv()
            if pair == 2:
                forward[number].start()
        mate_copies += forward
    for copy in mate_copies:
        copy.wait_recv()
    for copy in sent + mate_copies:
        copy.wait_send()
    for copy in own:
        copy.wait()


def gather_keys(kv, docs, queries, query_gain, cosine_table, sine_table, routes, size, capacity):
    pair = 2 if size % 2 == 0 else 1
    slots = max(size - 1, 1)
    rows, width = queries.shape
    return pl.pallas_call(
        functools.partial(gather_kernel, size, pair, capacity),
        out_shape=(
            jax.ShapeDtypeStruct((size,) + kv.shape, kv.dtype),
            jax.ShapeDtypeStruct((size,) + docs.shape, docs.dtype),
            jax.ShapeDtypeStruct((width // HEAD, rows, HEAD), jnp.bfloat16),
            jax.ShapeDtypeStruct(routes.shape, jnp.int32),
            jax.ShapeDtypeStruct(routes.shape[::-1], jnp.int32),
        ),
        in_specs=[ANY, ANY] + [VMEM] * 5,
        out_specs=(ANY, ANY, VMEM, VMEM, VMEM),
        scratch_shapes=[
            pltpu.SemaphoreType.DMA((slots, kv.shape[0])),
            pltpu.SemaphoreType.DMA((slots, kv.shape[0])),
            pltpu.SemaphoreType.DMA((slots,)),
            pltpu.SemaphoreType.DMA((slots,)),
            pltpu.SemaphoreType.DMA((2,)),
        ],
        compiler_params=pltpu.CompilerParams(collective_id=0, has_side_effects=True),
    )(kv, docs, queries, query_gain[None, :], cosine_table, sine_table, routes)


def attention_kernel(grouped, q_ref, qdoc_ref, kv_ref, doc_ref, scalar_ref, o_ref, m_ref, l_ref, acc_ref):
    rows = q_ref.shape[1]
    block = kv_ref.shape[2]
    pieces = doc_ref.shape[1]
    chunk = 256
    m_ref[...] = jnp.full(m_ref.shape, -1e30, jnp.float32)
    l_ref[...] = jnp.zeros(l_ref.shape, jnp.float32)
    acc_ref[...] = jnp.zeros(acc_ref.shape, jnp.float32)

    def advance(number, unused):
        keys = kv_ref[number, 0]
        values = kv_ref[number, 1]
        doc_rows = doc_ref[number]
        key_docs = jnp.concatenate([doc_rows[i : i + 1] for i in range(pieces)], axis=1)
        for head in range(grouped):
            for first in range(0, rows, chunk):
                part = pl.ds(first, chunk)
                scores = lax.dot_general(
                    q_ref[head, part],
                    keys,
                    (((1,), (1,)), ((), ())),
                    preferred_element_type=jnp.float32,
                )
                allowed = qdoc_ref[part, 0:1] == key_docs
                scores = jnp.where(allowed, scores * score_factor, -1e30)
                old_max = m_ref[head, part]
                new_max = jnp.maximum(old_max, jnp.max(scores, axis=1, keepdims=True))
                base = jnp.maximum(new_max[:, 0:1], -1e29)
                weights = jnp.exp2(scores - base)
                rescale = jnp.exp2(old_max - new_max)
                l_ref[head, part] = l_ref[head, part] * rescale + jnp.sum(
                    weights, axis=1, keepdims=True
                )
                acc_ref[head, part] = acc_ref[head, part] * rescale + jnp.dot(
                    weights.astype(jnp.bfloat16), values, preferred_element_type=jnp.float32
                )
                m_ref[head, part] = new_max
        return unused

    mine = lax.axis_index("sp")
    first_doc = scalar_ref[mine, 0, 0]
    last_doc = scalar_ref[mine, pieces - 1, HEAD - 1]

    def count(number, bounds):
        low, high = bounds
        low = low + (scalar_ref[number, pieces - 1, HEAD - 1] < first_doc).astype(jnp.int32)
        high = high + (scalar_ref[number, 0, 0] <= last_doc).astype(jnp.int32)
        return low, high

    low, high = lax.fori_loop(0, doc_ref.shape[0], count, (jnp.int32(0), jnp.int32(0)))
    lax.fori_loop(low, high, advance, 0)
    for head in range(grouped):
        o_ref[:, head * HEAD : (head + 1) * HEAD] = (acc_ref[head] / l_ref[head]).astype(
            o_ref.dtype
        )


def attend(query_rot, query_docs, kv_all, doc_all):
    grouped, rows, width = query_rot.shape
    return pl.pallas_call(
        functools.partial(attention_kernel, grouped),
        out_shape=jax.ShapeDtypeStruct((rows, grouped * width), jnp.bfloat16),
        in_specs=[VMEM, VMEM, VMEM, VMEM, SMEM],
        out_specs=VMEM,
        scratch_shapes=[pltpu.VMEM((grouped, rows, width), jnp.float32) for unused in range(3)],
        compiler_params=pltpu.CompilerParams(vmem_limit_bytes=48 * 1024 * 1024),
    )(query_rot, query_docs, kv_all, doc_all, doc_all)


def head_exchange_kernel(size, x_ref, o_ref, send_sem, recv_sem, own_sem):
    me = lax.axis_index("tp")
    rows, width = o_ref.shape[0], x_ref.shape[1]
    mine = o_ref.at[:, pl.ds(pl.multiple_of(me * width, width), width)]
    own = pltpu.make_async_copy(
        x_ref.at[pl.ds(pl.multiple_of(me * rows, rows), rows)], mine, own_sem
    )
    own.start()
    targets = [lax.rem(me + step, size) for step in range(1, size)]
    barrier_with([{"tp": target} for target in targets])
    copies = []
    for step, target in enumerate(targets):
        copy = pltpu.make_async_remote_copy(
            src_ref=x_ref.at[pl.ds(pl.multiple_of(target * rows, rows), rows)],
            dst_ref=mine,
            send_sem=send_sem.at[step],
            recv_sem=recv_sem.at[step],
            device_id={"tp": target},
            device_id_type=pl.DeviceIdType.MESH,
        )
        copy.start()
        copies.append(copy)
    for copy in copies:
        copy.wait()
    own.wait()


def exchange_heads(attention, size):
    rows, width = attention.shape
    return pl.pallas_call(
        functools.partial(head_exchange_kernel, size),
        out_shape=jax.ShapeDtypeStruct((rows // size, width * size), attention.dtype),
        in_specs=[VMEM],
        out_specs=VMEM,
        scratch_shapes=[
            pltpu.SemaphoreType.DMA((size,)),
            pltpu.SemaphoreType.DMA((size,)),
            pltpu.SemaphoreType.DMA,
        ],
        compiler_params=pltpu.CompilerParams(collective_id=1, has_side_effects=True),
    )(attention)


def expert_kernel(
    outer_size,
    inner_size,
    tp_size,
    x_ref,
    gate_ref,
    up_ref,
    down_ref,
    o_ref,
    held,
    served,
    out_send,
    out_recv,
    back_send,
    back_recv,
    own_sem,
):
    me = lax.axis_index("sp") * tp_size + lax.axis_index("tp")
    outer = me // inner_size
    inner = lax.rem(me, inner_size)
    size = outer_size * inner_size
    paired = outer_size & (outer_size - 1) == 0
    half = outer_size // 2
    upper, lower = list(range(half, outer_size)), list(range(1, half))
    if outer_size == 1:
        send_order, work_order = [0], [0]
    else:
        send_order = [group for group in upper + lower if group] + [0]
        work_order = [0] + [group for group in upper[:1] + lower + upper[1:] if group]

    def mesh_place(index):
        return {"sp": index // tp_size, "tp": lax.rem(index, tp_size)}

    def plane_to(group):
        if paired:
            return flipped(outer, group)
        return lax.rem(outer + group, outer_size)

    def plane_from(group):
        if paired:
            return flipped(outer, group)
        return lax.rem(outer - group + outer_size, outer_size)

    def target_of(group, step):
        return plane_to(group) * inner_size + lax.rem(inner + step, inner_size)

    def source_of(group, step):
        return plane_from(group) * inner_size + lax.rem(inner - step + inner_size, inner_size)

    def out_copy(group, step):
        target = target_of(group, step)
        return pltpu.make_async_remote_copy(
            src_ref=x_ref.at[target],
            dst_ref=held.at[me],
            send_sem=out_send.at[group * inner_size + step],
            recv_sem=out_recv.at[group * inner_size + step],
            device_id=mesh_place(target),
            device_id_type=pl.DeviceIdType.MESH,
        )

    def back_copy(group, step):
        source = source_of(group, step)
        return pltpu.make_async_remote_copy(
            src_ref=served.at[source],
            dst_ref=o_ref.at[me],
            send_sem=back_send.at[group * inner_size + step],
            recv_sem=back_recv.at[group * inner_size + step],
            device_id=mesh_place(source),
            device_id_type=pl.DeviceIdType.MESH,
        )

    def each(group, act):
        def once(step, unused):
            act(group, step)
            return unused

        lax.fori_loop(1 if group == 0 else 0, inner_size, once, 0)

    own_out = pltpu.make_async_copy(x_ref.at[me], held.at[me], own_sem.at[0])
    own_out.start()
    barrier = pltpu.get_barrier_semaphore()

    def greet(group, step):
        pl.semaphore_signal(
            barrier,
            inc=1,
            device_id=mesh_place(target_of(group, step)),
            device_id_type=pl.DeviceIdType.MESH,
        )

    for group in send_order:
        each(group, greet)
    pl.semaphore_wait(barrier, size - 1)
    for group in send_order:
        each(group, lambda g, step: out_copy(g, step).start())
    own_out.wait()
    local_experts = gate_ref.shape[0]
    block = held.shape[1]
    capacity = block // local_experts
    width = held.shape[2]
    for group in work_order:
        each(group, lambda g, step: out_copy(g, step).wait_recv())
        span = pl.ds(plane_from(group) * inner_size, inner_size)
        arrived = held[span]
        for expert in range(local_experts):
            part = slice(expert * capacity, (expert + 1) * capacity)
            rows = arrived[:, part].reshape(inner_size * capacity, width)
            gate = jnp.dot(rows, gate_ref[expert], preferred_element_type=jnp.float32)
            up = jnp.dot(rows, up_ref[expert], preferred_element_type=jnp.float32)
            hidden = (gate / (1.0 + jnp.exp(-gate)) * up).astype(jnp.bfloat16)
            result = jnp.dot(hidden, down_ref[expert], preferred_element_type=jnp.float32)
            served[span, part] = result.astype(jnp.bfloat16).reshape(inner_size, capacity, width)
        each(group, lambda g, step: back_copy(g, step).start())
    own_back = pltpu.make_async_copy(served.at[me], o_ref.at[me], own_sem.at[1])
    own_back.start()
    for group in work_order:
        each(group, lambda g, step: back_copy(g, step).wait_recv())
    for group in work_order:
        each(group, lambda g, step: out_copy(g, step).wait_send())
        each(group, lambda g, step: back_copy(g, step).wait_send())
    own_back.wait()


def run_experts(blocks, gate, up, down, sp_size, tp_size):
    size = blocks.shape[0]
    pair = 2 if sp_size % 2 == 0 else 1
    return pl.pallas_call(
        functools.partial(expert_kernel, sp_size // pair, pair * tp_size, tp_size),
        out_shape=jax.ShapeDtypeStruct(blocks.shape, blocks.dtype),
        in_specs=[VMEM] * 4,
        out_specs=VMEM,
        scratch_shapes=[pltpu.VMEM(blocks.shape, blocks.dtype) for unused in range(2)]
        + [pltpu.SemaphoreType.DMA((size,)) for unused in range(4)]
        + [pltpu.SemaphoreType.DMA((2,))],
        compiler_params=pltpu.CompilerParams(
            collective_id=2, has_side_effects=True, vmem_limit_bytes=48 * 1024 * 1024
        ),
    )(blocks, gate, up, down)


def middle_kernel(
    x_ref, gain_ref, proj_ref, res_ref, mid_gain_ref, mid_bias_ref, target_ref, mid_ref, out_ref
):
    whole = x_ref[...].astype(jnp.float32)
    mean_square = jnp.mean(whole * whole, axis=1, keepdims=True)
    scaled = (whole * gain_ref[...]).astype(jnp.bfloat16)
    projected = jnp.dot(scaled, proj_ref[...], preferred_element_type=jnp.float32)
    projected = projected * lax.rsqrt(mean_square + eps_norm)
    stream = alpha_mix * res_ref[...].astype(jnp.float32) + projected
    middle = layer_norm(stream, mid_gain_ref[...], mid_bias_ref[...]).astype(jnp.bfloat16)
    mid_ref[...] = middle
    slots, rows = out_ref.shape[0], middle.shape[0]
    slot = lax.broadcasted_iota(jnp.int32, (slots, rows), 0)
    chosen = slot == target_ref[0:1, :]
    for route in range(1, target_ref.shape[0]):
        chosen = chosen | (slot == target_ref[route : route + 1, :])
    select = jnp.where(chosen, 1.0, 0.0).astype(jnp.bfloat16)
    out_ref[...] = jnp.dot(select, middle, preferred_element_type=jnp.float32).astype(
        jnp.bfloat16
    )


def final_kernel(back_ref, target_ref, weight_ref, mid_ref, gain_ref, bias_ref, o_ref):
    rows, slots = mid_ref.shape[0], back_ref.shape[0]
    slot = lax.broadcasted_iota(jnp.int32, (rows, slots), 1)
    routed = None
    for route in range(target_ref.shape[1]):
        select = jnp.where(slot == target_ref[:, route : route + 1], 1.0, 0.0)
        picked = jnp.dot(
            select.astype(jnp.bfloat16), back_ref[...], preferred_element_type=jnp.float32
        )
        term = picked * weight_ref[:, route : route + 1]
        routed = term if routed is None else routed + term
    stream = alpha_mix * mid_ref[...].astype(jnp.float32) + routed
    o_ref[...] = layer_norm(stream, gain_ref[...], bias_ref[...]).astype(o_ref.dtype)


def per_device(
    queries,
    key_heads,
    value_heads,
    documents,
    query_gain,
    key_gain,
    out_gain,
    out_proj,
    residual,
    mid_gain,
    mid_bias,
    routes,
    route_weights,
    expert_gate,
    expert_up,
    expert_down,
    final_gain,
    final_bias,
):
    tok_rows = queries.shape[0]
    query_local = queries.shape[1] // HEAD
    key_local = key_heads.shape[1] // HEAD
    grouped = query_local // key_local
    sp_size = lax.axis_size("sp")
    tp_size = lax.axis_size("tp")
    offset = lax.axis_index("sp") * tok_rows
    cosine_table, sine_table = rotary_tables(tok_rows, offset)
    key_rot = normed_rotated(
        key_heads.reshape(tok_rows, key_local, HEAD), key_gain, cosine_table, sine_table
    )
    values = value_heads.reshape(tok_rows, key_local, HEAD)
    query_docs = jnp.broadcast_to(documents[:, None], (tok_rows, HEAD))
    kv = jnp.transpose(jnp.stack([key_rot, values]), (2, 0, 1, 3))
    out_rows, model_width = residual.shape
    top_count = routes.shape[1]
    local_experts = expert_gate.shape[0]
    device_total = sp_size * tp_size
    expert_total = local_experts * device_total
    capacity = 2 * out_rows * top_count // expert_total
    kv_all, doc_all, query_rot, target_columns, target_rows = gather_keys(
        kv.reshape(key_local * 2, tok_rows, HEAD),
        documents.reshape(tok_rows // HEAD, HEAD),
        queries,
        query_gain,
        cosine_table,
        sine_table,
        routes,
        sp_size,
        capacity,
    )
    heads = []
    for head in range(key_local):
        heads.append(
            attend(
                query_rot[head * grouped : (head + 1) * grouped],
                query_docs,
                kv_all if key_local == 1 else kv_all[:, 2 * head : 2 * head + 2],
                doc_all,
            )
        )
    attention = heads[0] if key_local == 1 else jnp.concatenate(heads, axis=1)
    whole_rows = exchange_heads(attention, tp_size)
    slots = expert_total * capacity
    middle, outbound = pl.pallas_call(
        middle_kernel,
        out_shape=(
            jax.ShapeDtypeStruct((out_rows, model_width), jnp.bfloat16),
            jax.ShapeDtypeStruct((slots, model_width), jnp.bfloat16),
        ),
        in_specs=[VMEM] * 7,
        out_specs=(VMEM, VMEM),
        compiler_params=pltpu.CompilerParams(vmem_limit_bytes=48 * 1024 * 1024),
    )(
        whole_rows,
        out_gain[None, :],
        out_proj,
        residual,
        mid_gain[None, :],
        mid_bias[None, :],
        target_rows,
    )
    returned = run_experts(
        outbound.reshape(device_total, local_experts * capacity, model_width),
        expert_gate,
        expert_up,
        expert_down,
        sp_size,
        tp_size,
    )
    return pl.pallas_call(
        final_kernel,
        out_shape=jax.ShapeDtypeStruct((out_rows, model_width), jnp.bfloat16),
        in_specs=[VMEM] * 6,
        out_specs=VMEM,
        compiler_params=pltpu.CompilerParams(vmem_limit_bytes=48 * 1024 * 1024),
    )(
        returned.reshape(slots, model_width),
        target_columns,
        route_weights,
        middle,
        final_gain[None, :],
        final_bias[None, :],
    )


def solution(mesh):
    return jax.shard_map(
        per_device,
        mesh=mesh,
        in_specs=(
            P("sp", "tp"),
            P("sp", "tp"),
            P("sp", "tp"),
            P("sp"),
            P(),
            P(),
            P(),
            P(),
            P(("sp", "tp"), None),
            P(),
            P(),
            P(("sp", "tp"), None),
            P(("sp", "tp"), None),
            P(("sp", "tp"), None, None),
            P(("sp", "tp"), None, None),
            P(("sp", "tp"), None, None),
            P(),
            P(),
        ),
        out_specs=P(("sp", "tp"), None),
        check_vma=False,
    )
```

profile of v0, /device:TPU:9, one launch (start us, length us, event | category | flops | bytes accessed | tf_op | source)
XLA Modules:
  0.0 182.1 jit_solution(7209993961277321560)
XLA Ops:
  0.0 0.0 copy-start.13
  0.0 0.0 copy-start.15
  0.0 0.2 broadcast_multiply_fusion.1
  0.2 1.1 fusion
  1.3 1.0 fusion.2
  2.4 0.0 copy-start.14
  2.4 1.2 fusion.3
  3.6 0.0 copy-done.13
  3.6 0.8 maximum_bitcast_fusion.kv_ref
  4.4 1.8 fusion.5
  6.2 0.0 copy-done.15
  6.2 0.7 copy.19.route_ref
  6.9 0.0 copy-start.3
  6.9 34.6 %shard_map.172 = (bf16[8,2,512,128]{3,2,1,0:T(8,128)(2,1)}, s32[8,4,128]{2,1,0:T(4,128)}, bf16[2,512,128]{2,1,0:T(8,128)(2,1)}, s32[128,2]{1,0:T(8,128)}, s32[2,128]{1,0:T(2,128)}) custom-call(bf16[2,512,128]{2,1,0:T(8,128)(2,1)} %maximum_bitcast_fusion.kv_ref, s32[4,128]{1,0:T(4,128)} %bitcast.30, bf16[512,256]{1,0:T(8,128)(2,1)} %q_ref.1, ...), custom_call_target="tpu_custom_call" | custom-call | tf_op jit(solution)/shard_map/pallas_call | solution.py:216
  41.6 0.0 copy-start.7
  41.6 0.0 copy-start.8
  41.6 0.0 copy-start.11
  41.6 0.0 copy-start.12
  41.6 0.0 copy-done.14
  41.7 0.1 broadcast_in_dim.15.qdoc_ref
  41.8 0.0 copy-start
  41.8 1.6 copy-done
  43.4 0.0 copy-start.4
  43.4 0.9 copy-done.4
  44.3 0.7 copy-done.5
  45.1 14.8 %shard_map.173.x_ref = bf16[512,256]{1,0:T(8,128)(2,1)S(1)} custom-call(bf16[2,512,128]{2,1,0:T(8,128)(2,1)S(1)} %copy-done.4, s32[512,128]{1,0:T(8,128)S(1)} %broadcast_in_dim.15.qdoc_ref, bf16[8,2,512,128]{3,2,1,0:T(8,128)(2,1)S(1)} %copy-done, s32[8,4,128]{2,1,0:T(4,128)S(1)} %copy-done.5, s32[8,4,128]{2,1,0:T(4,128)S(1)} %copy-done.5), custom_call_target="tpu_custom_call" | custom-call | tf_op jit(solution)/shard_map/pallas_call | solution.py:297
  59.8 0.0 copy-start.1
  59.9 0.7 copy-done.1
  60.5 8.6 %shard_map.174.x_ref = bf16[128,1024]{1,0:T(8,128)(2,1)} custom-call(bf16[512,256]{1,0:T(8,128)(2,1)} %copy-done.1), custom_call_target="tpu_custom_call" | custom-call | tf_op jit(solution)/shard_map/pallas_call | solution.py:336
  69.1 0.0 copy-done.3
  69.1 0.0 copy-done.7
  69.1 0.0 copy-done.8
  69.1 0.0 copy-done.11
  69.2 0.0 copy-done.12
  69.2 0.0 copy-start.2
  69.2 0.9 copy-done.2
  70.1 3.9 %shard_map.175 = (bf16[128,2048]{1,0:T(8,128)(2,1)S(1)}, bf16[512,2048]{1,0:T(8,128)(2,1)S(1)}) custom-call(bf16[128,1024]{1,0:T(8,128)(2,1)S(1)} %copy-done.2, f32[1,1024]{1,0:T(1,128)S(1)} %bitcast.28, bf16[1024,2048]{1,0:T(8,128)(2,1)} %proj_ref.1, bf16[128,2048]{1,0:T(8,128)(2,1)S(1)} %copy-done.3, f32[1,2048]{1,0:T(1,128)S(1)} %bitcast.24, ...), custom_call_target="tpu_custom_call" | custom-call | tf_op jit(solution)/shard_map/pallas_call | solution.py:591
  74.0 0.0 copy-start.16
  74.0 0.0 copy-start.6
  74.0 0.0 copy-start.9
  74.1 0.0 copy-start.10
  74.1 105.9 %shard_map.176 = bf16[32,16,2048]{2,1,0:T(8,128)(2,1)S(1)} custom-call(bf16[32,16,2048]{2,1,0:T(8,128)(2,1)S(1)} %bitcast.23, bf16[1,2048,512]{2,1,0:T(8,128)(2,1)} %gate_ref.1, bf16[1,2048,512]{2,1,0:T(8,128)(2,1)} %up_ref.1, bf16[1,512,2048]{2,1,0:T(8,128)(2,1)} %down_ref.1), custom_call_target="tpu_custom_call" | custom-call | tf_op jit(solution)/shard_map/pallas_call | solution.py:476
  180.0 0.0 copy-done.16
  180.0 0.1 copy.20.weight_ref
  180.1 0.0 copy-done.6
  180.1 0.0 copy-done.9
  180.1 0.0 copy-done.10
  180.1 2.0 %shard_map.177 = bf16[128,2048]{1,0:T(8,128)(2,1)} custom-call(bf16[512,2048]{1,0:T(8,128)(2,1)S(1)} %bitcast.22, s32[128,2]{1,0:T(8,128)S(1)} %copy-done.6, f32[128,2]{1,0:T(8,128)S(1)} %copy.20.weight_ref, bf16[128,2048]{1,0:T(8,128)(2,1)S(1)} %get-tuple-element.18.mid_ref, f32[1,2048]{1,0:T(1,128)S(1)} %bitcast.26, f32[1,2048]{1,0:T(1,128)S(1)} %bitcast.27), custom_call_target="tpu_custom_call" | custom-call | tf_op jit(solution)/shard_map/pallas_call | solution.py:617
  (4 shorter events, 0.0 us)
Async XLA Ops:
  0.0 3.6 %copy-start.13 = (bf16[512,128]{1,0:T(8,128)(2,1)S(1)}, bf16[512,128]{1,0:T(8,128)(2,1)}, u32[]{:S(2)}) copy-start(bf16[512,128]{1,0:T(8,128)(2,1)} %param.20) | copy-start | bytes 393220
  0.0 6.2 %copy-start.15 = (s32[128,2]{0,1:T(2,128)S(1)}, s32[128,2]{0,1:T(2,128)}, u32[]{:S(2)}) copy-start(s32[128,2]{0,1:T(2,128)} %param.29) | copy-start | bytes 3076
  2.4 39.3 %copy-start.14 = (s32[512]{0:T(512)S(1)}, s32[512]{0:T(512)}, u32[]{:S(2)}) copy-start(s32[512]{0:T(512)} %param.21) | copy-start | bytes 6148
  6.9 62.2 %copy-start.3 = (bf16[128,2048]{1,0:T(8,128)(2,1)S(1)}, bf16[128,2048]{1,0:T(8,128)(2,1)}, u32[]{:S(2)}) copy-start(bf16[128,2048]{1,0:T(8,128)(2,1)} %res_ref.1) | copy-start | bytes 1572868
  41.6 27.5 %copy-start.7 = (f32[2048]{0:T(1024)S(1)}, f32[2048]{0:T(1024)}, u32[]{:S(2)}) copy-start(f32[2048]{0:T(1024)} %param.27) | copy-start | bytes 24580
  41.6 27.5 %copy-start.8 = (f32[2048]{0:T(1024)S(1)}, f32[2048]{0:T(1024)}, u32[]{:S(2)}) copy-start(f32[2048]{0:T(1024)} %param.28) | copy-start | bytes 24580
  41.6 27.5 %copy-start.11 = (f32[1024]{0:T(1024)S(1)}, f32[1024]{0:T(1024)}, u32[]{:S(2)}) copy-start(f32[1024]{0:T(1024)} %param.24) | copy-start | bytes 12292
  41.6 27.5 %copy-start.12 = (s32[2,128]{1,0:T(2,128)S(1)}, s32[2,128]{1,0:T(2,128)}, u32[]{:S(2)}) copy-start(s32[2,128]{1,0:T(2,128)} %get-tuple-element.15.target_ref) | copy-start | bytes 3076
  41.8 1.6 copy-start
  43.4 0.9 copy-start.4
  44.3 0.7 copy-start.5
  59.8 0.7 copy-start.1
  69.2 1.0 copy-start.2
  74.0 105.9 %copy-start.16 = (f32[128,2]{0,1:T(2,128)S(1)}, f32[128,2]{0,1:T(2,128)}, u32[]{:S(2)}) copy-start(f32[128,2]{0,1:T(2,128)} %param.30) | copy-start | bytes 3076
  74.0 106.0 %copy-start.6 = (s32[128,2]{1,0:T(8,128)S(1)}, s32[128,2]{1,0:T(8,128)}, u32[]{:S(2)}) copy-start(s32[128,2]{1,0:T(8,128)} %get-tuple-element.17.target_ref) | copy-start | bytes 3076
  74.0 106.0 %copy-start.9 = (f32[2048]{0:T(1024)S(1)}, f32[2048]{0:T(1024)}, u32[]{:S(2)}) copy-start(f32[2048]{0:T(1024)} %param.34) | copy-start | bytes 24580
  74.1 106.0 %copy-start.10 = (f32[2048]{0:T(1024)S(1)}, f32[2048]{0:T(1024)}, u32[]{:S(2)}) copy-start(f32[2048]{0:T(1024)} %param.35) | copy-start | bytes 24580
where the time goes:
time: 183 us; the launch traced here: 182 us
  Pallas kernels  170 us (93%)
  other arithmetic  6.13 us (3%)
  local copies, waits for them, and re-layouts  5.94 us (3%)
    pallas_call x1, Pallas kernels, run_experts(): pl.pallas_call(functools.partial(expert_kernel, sp_size // pair, pair * t...  106 us
    pallas_call x1, Pallas kernels, gather_keys(): pl.pallas_call(functools.partial(gather_kernel, size, pair, capacity), ou...  34.6 us
    pallas_call x1, Pallas kernels, attend(): pl.pallas_call(functools.partial(attention_kernel, grouped), out_shape=ja...  14.8 us
    pallas_call x1, Pallas kernels, exchange_heads(): pl.pallas_call(functools.partial(head_exchange_kernel, size), out_shape=j...  8.55 us
    unnamed x36, local copies, waits for them, and re-layouts  5.82 us
    pallas_call x1, Pallas kernels, per_device(): pl.pallas_call(middle_kernel, out_shape=(jax.ShapeDtypeStruct((out_rows,...  3.9 us

commit v1 on v0

v1 whole, which is shorter than its diff:
```python
import functools

import jax
import jax.numpy as jnp
from jax import lax
from jax.experimental import pallas as pl
from jax.experimental.pallas import tpu as pltpu
from jax.sharding import PartitionSpec as P

HEAD = 128
GRID = 64


eps_norm = 1e-06
alpha_mix = 8.0**0.25
theta_base = 10000.0
score_factor = HEAD ** (-0.5) * 1.4426950408889634
VMEM = pl.BlockSpec(memory_space=pltpu.VMEM)
ANY = pl.BlockSpec(memory_space=pl.ANY)
SMEM = pl.BlockSpec(memory_space=pltpu.SMEM)


def layer_norm(stream, gain_vec, bias_vec):
    center = jnp.mean(stream, axis=-1, keepdims=True)
    spread = jnp.mean(jnp.square(stream - center), axis=-1, keepdims=True)
    return (stream - center) * lax.rsqrt(spread + eps_norm) * gain_vec + bias_vec


def flipped(number, pattern):
    bit = 1
    while bit <= pattern:
        if pattern & bit:
            number = number + bit - 2 * bit * lax.rem(number // bit, 2)
        bit *= 2
    return number


def turned(values, gain, cosine, sine):
    inv_rms = lax.rsqrt(jnp.mean(values * values, axis=1, keepdims=True) + eps_norm)
    values = values * inv_rms * gain
    return (values * cosine + pltpu.roll(values, HEAD // 2, 1) * sine).astype(jnp.bfloat16)


def front_kernel(
    size,
    pair,
    tp_size,
    capacity,
    q_ref,
    k_ref,
    v_ref,
    doc_ref,
    qdoc_ref,
    q_gain_ref,
    k_gain_ref,
    row_ref,
    col_ref,
    route_ref,
    gain_ref,
    proj_hbm,
    res_ref,
    mid_gain_ref,
    mid_bias_ref,
    mid_ref,
    out_ref,
    column_ref,
    kv,
    docs,
    q_rot,
    m_ref,
    l_ref,
    acc_ref,
    o_buf,
    whole,
    proj,
    line_send,
    line_recv,
    mate_send,
    mate_recv,
    tp_send,
    tp_recv,
    own_sem,
):
    me = lax.axis_index("sp")
    lane = lax.axis_index("tp")
    inner = lax.rem(me, pair)
    outer = me // pair
    steps = size // pair
    mate = outer * pair + lax.rem(inner + 1, pair)
    rows = k_ref.shape[0]
    pieces = doc_ref.shape[0]
    grouped = q_rot.shape[0]
    parts = 3

    load = pltpu.make_async_copy(proj_hbm, proj, own_sem.at[0])
    load.start()
    own = [
        pltpu.make_async_copy(v_ref, kv.at[me, 1], own_sem.at[1]),
        pltpu.make_async_copy(doc_ref, docs.at[me], own_sem.at[2]),
    ]
    for copy in own:
        copy.start()

    def on_line(place):
        return (place >= 0) & (place < steps)

    barrier = pltpu.get_barrier_semaphore()

    def greet(target):
        pl.semaphore_signal(
            barrier, inc=1, device_id=target, device_id_type=pl.DeviceIdType.MESH
        )

    peers = jnp.int32(tp_size - 1 + (pair - 1))
    for sign in (1, -1):
        there = on_line(outer + sign)
        pl.when(there)(lambda sign=sign: greet({"sp": (outer + sign) * pair + inner}))
        peers = peers + there.astype(jnp.int32)
    if pair == 2:
        greet({"sp": mate})
    tp_targets = [lax.rem(lane + step, tp_size) for step in range(1, tp_size)]
    for target in tp_targets:
        greet({"tp": target})
    pl.semaphore_wait(barrier, peers)

    def piece(place, part, first):
        if part == 2:
            return (doc_ref if first else docs.at[place]), docs.at[place]
        return (v_ref if first and part == 1 else kv.at[place, part]), kv.at[place, part]

    def line_copy(way, step, part, first=False):
        sign = 1 - 2 * way
        place = (outer - sign * (step - 1)) * pair + inner
        src, dst = piece(place, part, first)
        return pltpu.make_async_remote_copy(
            src_ref=src,
            dst_ref=dst,
            send_sem=line_send.at[way, step, part],
            recv_sem=line_recv.at[way, step, part],
            device_id={"sp": (outer + sign) * pair + inner},
            device_id_type=pl.DeviceIdType.MESH,
        )

    def mate_copy(way, step, part, first=False):
        sign = 1 - 2 * way
        place = (outer - sign * step) * pair + inner
        src, dst = piece(place, part, first)
        return pltpu.make_async_remote_copy(
            src_ref=src,
            dst_ref=dst,
            send_sem=mate_send.at[way, step, part],
            recv_sem=mate_recv.at[way, step, part],
            device_id={"sp": mate},
            device_id_type=pl.DeviceIdType.MESH,
        )

    def send_own(part):
        for way in range(2):
            pl.when(on_line(outer + 1 - 2 * way))(
                lambda way=way: line_copy(way, 1, part, True).start()
            )
        if pair == 2:
            mate_copy(0, 0, part, True).start()

    send_own(1)
    send_own(2)
    grid_rows = row_ref.shape[1]
    span = col_ref.shape[1]

    def tables(block):
        cosine = row_ref[0, pl.ds(block, 1)] + col_ref[0]
        sine = row_ref[1, pl.ds(block, 1)] + col_ref[1]
        return cosine, sine

    def turn_keys(block, unused):
        cosine, sine = tables(block)
        here = pl.ds(pl.multiple_of(block * span, span), span)
        kv[me, 0, here] = turned(k_ref[here].astype(jnp.float32), k_gain_ref[...], cosine, sine)
        return unused

    lax.fori_loop(0, grid_rows, turn_keys, 0)
    send_own(0)

    def turn_queries(block, unused):
        cosine, sine = tables(block)
        here = pl.ds(pl.multiple_of(block * span, span), span)
        for head in range(grouped):
            q_rot[head, here] = turned(
                q_ref[here, head * HEAD : (head + 1) * HEAD].astype(jnp.float32),
                q_gain_ref[...],
                cosine,
                sine,
            )
        return unused

    lax.fori_loop(0, grid_rows, turn_queries, 0)
    m_ref[...] = jnp.full(m_ref.shape, -1e30, jnp.float32)
    l_ref[...] = jnp.zeros(l_ref.shape, jnp.float32)
    acc_ref[...] = jnp.zeros(acc_ref.shape, jnp.float32)
    for copy in own:
        copy.wait()
    chunk = 256

    def advance(place):
        keys = kv[place, 0]
        values = kv[place, 1]
        doc_rows = docs[place]
        key_docs = jnp.concatenate([doc_rows[i : i + 1] for i in range(pieces)], axis=1)
        for head in range(grouped):
            for first in range(0, rows, chunk):
                part = pl.ds(first, chunk)
                scores = lax.dot_general(
                    q_rot[head, part],
                    keys,
                    (((1,), (1,)), ((), ())),
                    preferred_element_type=jnp.float32,
                )
                allowed = qdoc_ref[part, 0:1] == key_docs
                scores = jnp.where(allowed, scores * score_factor, -1e30)
                old_max = m_ref[head, part]
                new_max = jnp.maximum(old_max, jnp.max(scores, axis=1, keepdims=True))
                base = jnp.maximum(new_max[:, 0:1], -1e29)
                weights = jnp.exp2(scores - base)
                rescale = jnp.exp2(old_max - new_max)
                l_ref[head, part] = l_ref[head, part] * rescale + jnp.sum(
                    weights, axis=1, keepdims=True
                )
                acc_ref[head, part] = acc_ref[head, part] * rescale + jnp.dot(
                    weights.astype(jnp.bfloat16), values, preferred_element_type=jnp.float32
                )
                m_ref[head, part] = new_max

    def stage(step, unused):
        for group in ((1, 2), (0,)):
            for way in range(2):
                sign = 1 - 2 * way

                def take(way=way, sign=sign, group=group):
                    for part in group:
                        line_copy(way, step, part).wait_recv()

                    def pass_on():
                        for part in group:
                            line_copy(way, step + 1, part).start()

                    pl.when(on_line(outer + sign))(pass_on)
                    if pair == 2:
                        for part in group:
                            mate_copy(way, step, part).start()

                pl.when((step > 0) & on_line(outer - sign * step))(take)

        def visit(number, unused):
            way = lax.rem(number, 2)
            across = number // 2
            there = outer - (1 - 2 * way) * step

            def work():
                if pair == 2:

                    def arrive():
                        for part in range(parts):
                            mate_copy(way, step, part).wait_recv()

                    pl.when(across == 1)(arrive)
                advance(there * pair + lax.rem(inner + across, pair))

            pl.when(on_line(there) & ((step > 0) | (way == 0)))(work)
            return unused

        lax.fori_loop(0, 2 * pair, visit, 0)
        return unused

    lax.fori_loop(0, steps, stage, 0)
    for head in range(grouped):
        o_buf[:, head * HEAD : (head + 1) * HEAD] = (acc_ref[head] / l_ref[head]).astype(
            o_buf.dtype
        )

    out_rows, width = whole.shape[0], o_buf.shape[1]

    def rows_of(number):
        return pl.ds(pl.multiple_of(number * out_rows, out_rows), out_rows)

    mine = whole.at[:, pl.ds(pl.multiple_of(lane * width, width), width)]
    swaps = []
    for step, target in enumerate(tp_targets):
        copy = pltpu.make_async_remote_copy(
            src_ref=o_buf.at[rows_of(target)],
            dst_ref=mine,
            send_sem=tp_send.at[step],
            recv_sem=tp_recv.at[step],
            device_id={"tp": target},
            device_id_type=pl.DeviceIdType.MESH,
        )
        copy.start()
        swaps.append(copy)
    keep = pltpu.make_async_copy(o_buf.at[rows_of(lane)], mine, own_sem.at[3])
    keep.start()

    top, tokens = route_ref.shape
    experts = 2 * tokens * top // capacity
    down = lax.broadcasted_iota(jnp.int32, (tokens, tokens), 0)
    over = lax.broadcasted_iota(jnp.int32, (tokens, tokens), 1)
    earlier = jnp.where(down < over, 1.0, 0.0).astype(jnp.bfloat16)
    names = lax.broadcasted_iota(jnp.int32, (experts, tokens), 0)
    passed = jnp.zeros((experts, 1), jnp.float32)
    slots = out_ref.shape[0]
    slot = lax.broadcasted_iota(jnp.int32, (slots, tokens), 0)
    chosen = None
    for route in range(top):
        named = route_ref[route : route + 1, :]
        one_hot = jnp.where(names == named, 1.0, 0.0)
        before = passed + jnp.dot(
            one_hot.astype(jnp.bfloat16), earlier, preferred_element_type=jnp.float32
        )
        rank = jnp.sum(before * one_hot, axis=0, keepdims=True)
        target = named.astype(jnp.float32) * capacity + rank
        column_ref[:, route : route + 1] = jnp.sum(
            jnp.where(down == over, target, 0.0), axis=1, keepdims=True
        ).astype(jnp.int32)
        passed = passed + jnp.sum(one_hot, axis=1, keepdims=True)
        match = slot == target.astype(jnp.int32)
        chosen = match if chosen is None else chosen | match
    select = jnp.where(chosen, 1.0, 0.0).astype(jnp.bfloat16)

    load.wait()
    for copy in swaps:
        copy.wait_recv()
    keep.wait()
    taken = whole[...].astype(jnp.float32)
    mean_square = jnp.mean(taken * taken, axis=1, keepdims=True)
    scaled = (taken * gain_ref[...]).astype(jnp.bfloat16)
    projected = jnp.dot(scaled, proj[...], preferred_element_type=jnp.float32)
    projected = projected * lax.rsqrt(mean_square + eps_norm)
    stream = alpha_mix * res_ref[...].astype(jnp.float32) + projected
    middle = layer_norm(stream, mid_gain_ref[...], mid_bias_ref[...]).astype(jnp.bfloat16)
    mid_ref[...] = middle
    out_ref[...] = jnp.dot(select, middle, preferred_element_type=jnp.float32).astype(
        jnp.bfloat16
    )

    for copy in swaps:
        copy.wait_send()

    def settle(step, unused):
        for way in range(2):
            sign = 1 - 2 * way

            def sent(way=way):
                for part in range(parts):
                    line_copy(way, step + 1, part).wait_send()

            pl.when(on_line(outer - sign * step) & on_line(outer + sign))(sent)
            if pair == 2:

                def gave(way=way):
                    for part in range(parts):
                        mate_copy(way, step, part).wait_send()

                first = (step > 0) | (way == 0)
                pl.when(on_line(outer - sign * step) & first)(gave)
        return unused

    lax.fori_loop(0, steps, settle, 0)


def trig_tables(tok_rows, offset):
    pair_count = HEAD // 4
    inv_freq = theta_base ** (-jnp.arange(pair_count, dtype=jnp.float32) / pair_count)
    grid_rows = (offset // GRID + jnp.arange(tok_rows // GRID, dtype=jnp.int32)).astype(jnp.float32)
    grid_cols = jnp.arange(GRID, dtype=jnp.int32).astype(jnp.float32)
    tables = []
    for at, place in enumerate((grid_rows, grid_cols)):
        angles = place[:, None] * inv_freq[None, :]
        blank = jnp.zeros_like(angles)
        cosine, sine = jnp.cos(angles), jnp.sin(angles)
        order = (lambda a, b: [a, blank, b, blank]) if at == 0 else (lambda a, b: [blank, a, blank, b])
        tables.append(
            jnp.stack(
                [
                    jnp.concatenate(order(cosine, cosine), axis=1),
                    jnp.concatenate(order(-sine, sine), axis=1),
                ]
            )
        )
    return tables


def run_front(
    queries,
    keys,
    values,
    documents,
    query_gain,
    key_gain,
    routes,
    out_gain,
    out_proj,
    residual,
    mid_gain,
    mid_bias,
    size,
    tp_size,
    capacity,
):
    pair = 2 if size % 2 == 0 else 1
    rows, width = queries.shape
    grouped = width // HEAD
    out_rows, model_width = residual.shape
    steps = size // pair
    row_table, col_table = trig_tables(rows, lax.axis_index("sp") * rows)
    query_docs = jnp.broadcast_to(documents[:, None], (rows, HEAD))
    slots = 2 * out_rows * routes.shape[1]
    dma = pltpu.SemaphoreType.DMA
    return pl.pallas_call(
        functools.partial(front_kernel, size, pair, tp_size, capacity),
        out_shape=(
            jax.ShapeDtypeStruct((out_rows, model_width), jnp.bfloat16),
            jax.ShapeDtypeStruct((slots, model_width), jnp.bfloat16),
            jax.ShapeDtypeStruct(routes.shape, jnp.int32),
        ),
        in_specs=[VMEM] * 11 + [ANY] + [VMEM] * 3,
        out_specs=(VMEM, VMEM, VMEM),
        scratch_shapes=[
            pltpu.VMEM((size, 2, rows, HEAD), jnp.bfloat16),
            pltpu.VMEM((size, rows // HEAD, HEAD), jnp.int32),
            pltpu.VMEM((grouped, rows, HEAD), jnp.bfloat16),
            pltpu.VMEM((grouped, rows, HEAD), jnp.float32),
            pltpu.VMEM((grouped, rows, HEAD), jnp.float32),
            pltpu.VMEM((grouped, rows, HEAD), jnp.float32),
            pltpu.VMEM((rows, width), jnp.bfloat16),
            pltpu.VMEM((out_rows, width * tp_size), jnp.bfloat16),
            pltpu.VMEM(out_proj.shape, out_proj.dtype),
            dma((2, steps + 1, 3)),
            dma((2, steps + 1, 3)),
            dma((2, steps, 3)),
            dma((2, steps, 3)),
            dma((tp_size,)),
            dma((tp_size,)),
            dma((4,)),
        ],
        compiler_params=pltpu.CompilerParams(
            collective_id=0, has_side_effects=True, vmem_limit_bytes=56 * 1024 * 1024
        ),
    )(
        queries,
        keys,
        values,
        documents.reshape(rows // HEAD, HEAD),
        query_docs,
        query_gain[None, :],
        key_gain[None, :],
        row_table,
        col_table,
        routes.T,
        out_gain[None, :],
        out_proj,
        residual,
        mid_gain[None, :],
        mid_bias[None, :],
    )


def expert_kernel(
    outer_size,
    inner_size,
    tp_size,
    x_ref,
    gate_ref,
    up_ref,
    down_ref,
    o_ref,
    held,
    served,
    out_send,
    out_recv,
    back_send,
    back_recv,
    own_sem,
):
    me = lax.axis_index("sp") * tp_size + lax.axis_index("tp")
    outer = me // inner_size
    inner = lax.rem(me, inner_size)
    size = outer_size * inner_size
    paired = outer_size & (outer_size - 1) == 0
    half = outer_size // 2
    upper, lower = list(range(half, outer_size)), list(range(1, half))
    if outer_size == 1:
        send_order, work_order = [0], [0]
    else:
        send_order = [group for group in upper + lower if group] + [0]
        work_order = [0] + [group for group in upper[:1] + lower + upper[1:] if group]

    def mesh_place(index):
        return {"sp": index // tp_size, "tp": lax.rem(index, tp_size)}

    def plane_to(group):
        if paired:
            return flipped(outer, group)
        return lax.rem(outer + group, outer_size)

    def plane_from(group):
        if paired:
            return flipped(outer, group)
        return lax.rem(outer - group + outer_size, outer_size)

    def target_of(group, step):
        return plane_to(group) * inner_size + lax.rem(inner + step, inner_size)

    def source_of(group, step):
        return plane_from(group) * inner_size + lax.rem(inner - step + inner_size, inner_size)

    def out_copy(group, step):
        target = target_of(group, step)
        return pltpu.make_async_remote_copy(
            src_ref=x_ref.at[target],
            dst_ref=held.at[me],
            send_sem=out_send.at[group * inner_size + step],
            recv_sem=out_recv.at[group * inner_size + step],
            device_id=mesh_place(target),
            device_id_type=pl.DeviceIdType.MESH,
        )

    def back_copy(group, step):
        source = source_of(group, step)
        return pltpu.make_async_remote_copy(
            src_ref=served.at[source],
            dst_ref=o_ref.at[me],
            send_sem=back_send.at[group * inner_size + step],
            recv_sem=back_recv.at[group * inner_size + step],
            device_id=mesh_place(source),
            device_id_type=pl.DeviceIdType.MESH,
        )

    def each(group, act):
        def once(step, unused):
            act(group, step)
            return unused

        lax.fori_loop(1 if group == 0 else 0, inner_size, once, 0)

    own_out = pltpu.make_async_copy(x_ref.at[me], held.at[me], own_sem.at[0])
    own_out.start()
    barrier = pltpu.get_barrier_semaphore()

    def greet(group, step):
        pl.semaphore_signal(
            barrier,
            inc=1,
            device_id=mesh_place(target_of(group, step)),
            device_id_type=pl.DeviceIdType.MESH,
        )

    for group in send_order:
        each(group, greet)
    pl.semaphore_wait(barrier, size - 1)
    for group in send_order:
        each(group, lambda g, step: out_copy(g, step).start())
    own_out.wait()
    local_experts = gate_ref.shape[0]
    block = held.shape[1]
    capacity = block // local_experts
    width = held.shape[2]
    for group in work_order:
        each(group, lambda g, step: out_copy(g, step).wait_recv())
        span = pl.ds(plane_from(group) * inner_size, inner_size)
        arrived = held[span]
        for expert in range(local_experts):
            part = slice(expert * capacity, (expert + 1) * capacity)
            rows = arrived[:, part].reshape(inner_size * capacity, width)
            gate = jnp.dot(rows, gate_ref[expert], preferred_element_type=jnp.float32)
            up = jnp.dot(rows, up_ref[expert], preferred_element_type=jnp.float32)
            hidden = (gate / (1.0 + jnp.exp(-gate)) * up).astype(jnp.bfloat16)
            result = jnp.dot(hidden, down_ref[expert], preferred_element_type=jnp.float32)
            served[span, part] = result.astype(jnp.bfloat16).reshape(inner_size, capacity, width)
        each(group, lambda g, step: back_copy(g, step).start())
    own_back = pltpu.make_async_copy(served.at[me], o_ref.at[me], own_sem.at[1])
    own_back.start()
    for group in work_order:
        each(group, lambda g, step: back_copy(g, step).wait_recv())
    for group in work_order:
        each(group, lambda g, step: out_copy(g, step).wait_send())
        each(group, lambda g, step: back_copy(g, step).wait_send())
    own_back.wait()


def run_experts(blocks, gate, up, down, sp_size, tp_size):
    size = blocks.shape[0]
    pair = 2 if sp_size % 2 == 0 else 1
    return pl.pallas_call(
        functools.partial(expert_kernel, sp_size // pair, pair * tp_size, tp_size),
        out_shape=jax.ShapeDtypeStruct(blocks.shape, blocks.dtype),
        in_specs=[VMEM] * 4,
        out_specs=VMEM,
        scratch_shapes=[pltpu.VMEM(blocks.shape, blocks.dtype) for unused in range(2)]
        + [pltpu.SemaphoreType.DMA((size,)) for unused in range(4)]
        + [pltpu.SemaphoreType.DMA((2,))],
        compiler_params=pltpu.CompilerParams(
            collective_id=2, has_side_effects=True, vmem_limit_bytes=48 * 1024 * 1024
        ),
    )(blocks, gate, up, down)


def final_kernel(back_ref, target_ref, weight_ref, mid_ref, gain_ref, bias_ref, o_ref):
    rows, slots = mid_ref.shape[0], back_ref.shape[0]
    slot = lax.broadcasted_iota(jnp.int32, (rows, slots), 1)
    routed = None
    for route in range(target_ref.shape[1]):
        select = jnp.where(slot == target_ref[:, route : route + 1], 1.0, 0.0)
        picked = jnp.dot(
            select.astype(jnp.bfloat16), back_ref[...], preferred_element_type=jnp.float32
        )
        term = picked * weight_ref[:, route : route + 1]
        routed = term if routed is None else routed + term
    stream = alpha_mix * mid_ref[...].astype(jnp.float32) + routed
    o_ref[...] = layer_norm(stream, gain_ref[...], bias_ref[...]).astype(o_ref.dtype)


def per_device(
    queries,
    key_heads,
    value_heads,
    documents,
    query_gain,
    key_gain,
    out_gain,
    out_proj,
    residual,
    mid_gain,
    mid_bias,
    routes,
    route_weights,
    expert_gate,
    expert_up,
    expert_down,
    final_gain,
    final_bias,
):
    sp_size = lax.axis_size("sp")
    tp_size = lax.axis_size("tp")
    if key_heads.shape[1] != HEAD or expert_gate.shape[0] != 1:
        raise ValueError("unsupported placement")
    out_rows, model_width = residual.shape
    local_experts = expert_gate.shape[0]
    device_total = sp_size * tp_size
    expert_total = local_experts * device_total
    capacity = 2 * out_rows * routes.shape[1] // expert_total
    slots = expert_total * capacity
    middle, outbound, target_columns = run_front(
        queries,
        key_heads,
        value_heads,
        documents,
        query_gain,
        key_gain,
        routes,
        out_gain,
        out_proj,
        residual,
        mid_gain,
        mid_bias,
        sp_size,
        tp_size,
        capacity,
    )
    returned = run_experts(
        outbound.reshape(device_total, local_experts * capacity, model_width),
        expert_gate,
        expert_up,
        expert_down,
        sp_size,
        tp_size,
    )
    return pl.pallas_call(
        final_kernel,
        out_shape=jax.ShapeDtypeStruct((out_rows, model_width), jnp.bfloat16),
        in_specs=[VMEM] * 6,
        out_specs=VMEM,
        compiler_params=pltpu.CompilerParams(vmem_limit_bytes=48 * 1024 * 1024),
    )(
        returned.reshape(slots, model_width),
        target_columns,
        route_weights,
        middle,
        final_gain[None, :],
        final_bias[None, :],
    )


def solution(mesh):
    return jax.shard_map(
        per_device,
        mesh=mesh,
        in_specs=(
            P("sp", "tp"),
            P("sp", "tp"),
            P("sp", "tp"),
            P("sp"),
            P(),
            P(),
            P(),
            P(),
            P(("sp", "tp"), None),
            P(),
            P(),
            P(("sp", "tp"), None),
            P(("sp", "tp"), None),
            P(("sp", "tp"), None, None),
            P(("sp", "tp"), None, None),
            P(("sp", "tp"), None, None),
            P(),
            P(),
        ),
        out_specs=P(("sp", "tp"), None),
        check_vma=False,
    )
```

time: 183 us -> 158 us (0.86)
  Pallas kernels: 170 us -> 152 us
  other arithmetic: 6.13 us -> 1.76 us
  local copies, waits for them, and re-layouts: 5.94 us -> 3.24 us
    pallas_call x4 -> x1, Pallas kernels: 61.9 us -> 45.2 us  [run_front(): pl.pallas_call(functools.partial(front_kernel, size, pair, tp_size, capac...]
    unnamed x36 -> x13, local copies, waits for them, and re-layouts: 5.82 us -> 1.72 us
where the time goes in v1:
time: 158 us; the launch traced here: 157 us
  Pallas kernels  152 us (96%)
  local copies, waits for them, and re-layouts  3.24 us (2%)
  other arithmetic  1.76 us (1%)
    pallas_call x1, Pallas kernels, run_experts(): pl.pallas_call(functools.partial(expert_kernel, sp_size // pair, pair * t...  105 us
    pallas_call x1, Pallas kernels, run_front(): pl.pallas_call(functools.partial(front_kernel, size, pair, tp_size, capac...  45.2 us

profile of v1, /device:TPU:9, one launch (start us, length us, event | category | flops | bytes accessed | tf_op | source)
XLA Modules:
  0.0 157.3 jit_solution(1902327318683419875)
XLA Ops:
  0.0 0.1 multiply_cosine_fusion.1
  0.1 0.1 fusion.7
  0.2 0.6 pad_maximum_fusion.5.row_ref
  0.8 0.2 multiply_cosine_fusion
  1.0 0.1 fusion.1
  1.2 0.6 pad_maximum_fusion.col_ref
  1.8 1.5 broadcast_in_dim.37.qdoc_ref
  3.3 45.2 %shard_map.172 = (bf16[128,2048]{1,0:T(8,128)(2,1)}, bf16[512,2048]{1,0:T(8,128)(2,1)}, s32[128,2]{1,0:T(8,128)}) custom-call(bf16[512,256]{1,0:T(8,128)(2,1)} %q_ref.1, bf16[512,128]{1,0:T(8,128)(2,1)} %k_ref.1, bf16[512,128]{1,0:T(8,128)(2,1)} %v_ref.1, s32[4,128]{1,0:T(4,128)} %bitcast.25, s32[512,128]{1,0:T(8,128)} %broadcast_in_dim.37.qdoc_ref, ...), custom_call_target="tpu_custom_call" | custom-call | tf_op jit(solution)/shard_map/pallas_call | solution.py:416
  48.5 0.0 copy-start
  48.5 1.6 %copy-done = bf16[512,2048]{1,0:T(8,128)(2,1)S(1)} copy-done((bf16[512,2048]{1,0:T(8,128)(2,1)S(1)}, bf16[512,2048]{1,0:T(8,128)(2,1)}, u32[]{:S(2)}) %copy-start) | copy-done | bytes 2097176
  50.1 0.0 copy-start.5
  50.1 0.0 copy-start.1
  50.1 0.0 copy-start.2
  50.1 0.0 copy-start.3
  50.1 0.0 copy-start.4
  50.1 105.1 %shard_map.173 = bf16[32,16,2048]{2,1,0:T(8,128)(2,1)S(1)} custom-call(bf16[32,16,2048]{2,1,0:T(8,128)(2,1)S(1)} %bitcast.20, bf16[1,2048,512]{2,1,0:T(8,128)(2,1)} %gate_ref.1, bf16[1,2048,512]{2,1,0:T(8,128)(2,1)} %up_ref.1, bf16[1,512,2048]{2,1,0:T(8,128)(2,1)} %down_ref.1), custom_call_target="tpu_custom_call" | custom-call | tf_op jit(solution)/shard_map/pallas_call | solution.py:591
  155.2 0.0 copy-done.5
  155.2 0.1 copy.19.weight_ref
  155.3 0.0 copy-done.1
  155.3 0.0 copy-done.2
  155.3 0.0 copy-done.3
  155.3 0.0 copy-done.4
  155.3 2.0 %shard_map.174 = bf16[128,2048]{1,0:T(8,128)(2,1)} custom-call(bf16[512,2048]{1,0:T(8,128)(2,1)S(1)} %bitcast.19, s32[128,2]{1,0:T(8,128)S(1)} %copy-done.2, f32[128,2]{1,0:T(8,128)S(1)} %copy.19.weight_ref, bf16[128,2048]{1,0:T(8,128)(2,1)S(1)} %copy-done.1, f32[1,2048]{1,0:T(1,128)S(1)} %bitcast.21, f32[1,2048]{1,0:T(1,128)S(1)} %bitcast.22), custom_call_target="tpu_custom_call" | custom-call | tf_op jit(solution)/shard_map/pallas_call | solution.py:675
  (5 shorter events, 0.0 us)
Async XLA Ops:
  48.5 1.6 %copy-start = (bf16[512,2048]{1,0:T(8,128)(2,1)S(1)}, bf16[512,2048]{1,0:T(8,128)(2,1)}, u32[]{:S(2)}) copy-start(bf16[512,2048]{1,0:T(8,128)(2,1)} %get-tuple-element.8) | copy-start | bytes 6291460
  50.1 105.1 %copy-start.5 = (f32[128,2]{0,1:T(2,128)S(1)}, f32[128,2]{0,1:T(2,128)}, u32[]{:S(2)}) copy-start(f32[128,2]{0,1:T(2,128)} %param.30) | copy-start | bytes 3076
  50.1 105.2 %copy-start.1 = (bf16[128,2048]{1,0:T(8,128)(2,1)S(1)}, bf16[128,2048]{1,0:T(8,128)(2,1)}, u32[]{:S(2)}) copy-start(bf16[128,2048]{1,0:T(8,128)(2,1)} %get-tuple-element.10.mid_ref) | copy-start | bytes 1572868
  50.1 105.2 %copy-start.2 = (s32[128,2]{1,0:T(8,128)S(1)}, s32[128,2]{1,0:T(8,128)}, u32[]{:S(2)}) copy-start(s32[128,2]{1,0:T(8,128)} %get-tuple-element.9.target_ref) | copy-start | bytes 3076
  50.1 105.2 %copy-start.3 = (f32[2048]{0:T(1024)S(1)}, f32[2048]{0:T(1024)}, u32[]{:S(2)}) copy-start(f32[2048]{0:T(1024)} %param.34) | copy-start | bytes 24580
  50.1 105.3 %copy-start.4 = (f32[2048]{0:T(1024)S(1)}, f32[2048]{0:T(1024)}, u32[]{:S(2)}) copy-start(f32[2048]{0:T(1024)} %param.35) | copy-start | bytes 24580

commit v2 on v1

--- a/solution.py
+++ b/solution.py
@@ -9,6 +9,7 @@
 
 HEAD = 128
 GRID = 64
+CHUNKS = 4
 
 
 eps_norm = 1e-06
@@ -26,15 +27,6 @@
     return (stream - center) * lax.rsqrt(spread + eps_norm) * gain_vec + bias_vec
 
 
-def flipped(number, pattern):
-    bit = 1
-    while bit <= pattern:
-        if pattern & bit:
-            number = number + bit - 2 * bit * lax.rem(number // bit, 2)
-        bit *= 2
-    return number
-
-
 def turned(values, gain, cosine, sine):
     inv_rms = lax.rsqrt(jnp.mean(values * values, axis=1, keepdims=True) + eps_norm)
     values = values * inv_rms * gain
@@ -45,7 +37,6 @@
     size,
     pair,
     tp_size,
-    capacity,
     q_ref,
     k_ref,
     v_ref,
@@ -55,15 +46,12 @@
     k_gain_ref,
     row_ref,
     col_ref,
-    route_ref,
     gain_ref,
     proj_hbm,
     res_ref,
     mid_gain_ref,
     mid_bias_ref,
     mid_ref,
-    out_ref,
-    column_ref,
     kv,
     docs,
     q_rot,
@@ -298,32 +286,6 @@
     keep = pltpu.make_async_copy(o_buf.at[rows_of(lane)], mine, own_sem.at[3])
     keep.start()
 
-    top, tokens = route_ref.shape
-    experts = 2 * tokens * top // capacity
-    down = lax.broadcasted_iota(jnp.int32, (tokens, tokens), 0)
-    over = lax.broadcasted_iota(jnp.int32, (tokens, tokens), 1)
-    earlier = jnp.where(down < over, 1.0, 0.0).astype(jnp.bfloat16)
-    names = lax.broadcasted_iota(jnp.int32, (experts, tokens), 0)
-    passed = jnp.zeros((experts, 1), jnp.float32)
-    slots = out_ref.shape[0]
-    slot = lax.broadcasted_iota(jnp.int32, (slots, tokens), 0)
-    chosen = None
-    for route in range(top):
-        named = route_ref[route : route + 1, :]
-        one_hot = jnp.where(names == named, 1.0, 0.0)
-        before = passed + jnp.dot(
-            one_hot.astype(jnp.bfloat16), earlier, preferred_element_type=jnp.float32
-        )
-        rank = jnp.sum(before * one_hot, axis=0, keepdims=True)
-        target = named.astype(jnp.float32) * capacity + rank
-        column_ref[:, route : route + 1] = jnp.sum(
-            jnp.where(down == over, target, 0.0), axis=1, keepdims=True
-        ).astype(jnp.int32)
-        passed = passed + jnp.sum(one_hot, axis=1, keepdims=True)
-        match = slot == target.astype(jnp.int32)
-        chosen = match if chosen is None else chosen | match
-    select = jnp.where(chosen, 1.0, 0.0).astype(jnp.bfloat16)
-
     load.wait()
     for copy in swaps:
         copy.wait_recv()
@@ -335,10 +297,9 @@
     projected = projected * lax.rsqrt(mean_square + eps_norm)
     stream = alpha_mix * res_ref[...].astype(jnp.float32) + projected
     middle = layer_norm(stream, mid_gain_ref[...], mid_bias_ref[...]).astype(jnp.bfloat16)
-    mid_ref[...] = middle
-    out_ref[...] = jnp.dot(select, middle, preferred_element_type=jnp.float32).astype(
-        jnp.bfloat16
-    )
+    block = mid_ref.shape[2]
+    for chunk in range(mid_ref.shape[0]):
+        mid_ref[chunk] = middle[:, chunk * block : (chunk + 1) * block]
 
     for copy in swaps:
         copy.wait_send()
@@ -394,7 +355,6 @@
     documents,
     query_gain,
     key_gain,
-    routes,
     out_gain,
     out_proj,
     residual,
@@ -402,7 +362,7 @@
     mid_bias,
     size,
     tp_size,
-    capacity,
+    chunks,
 ):
     pair = 2 if size % 2 == 0 else 1
     rows, width = queries.shape
@@ -411,17 +371,12 @@
     steps = size // pair
     row_table, col_table = trig_tables(rows, lax.axis_index("sp") * rows)
     query_docs = jnp.broadcast_to(documents[:, None], (rows, HEAD))
-    slots = 2 * out_rows * routes.shape[1]
     dma = pltpu.SemaphoreType.DMA
     return pl.pallas_call(
-        functools.partial(front_kernel, size, pair, tp_size, capacity),
-        out_shape=(
-            jax.ShapeDtypeStruct((out_rows, model_width), jnp.bfloat16),
-            jax.ShapeDtypeStruct((slots, model_width), jnp.bfloat16),
-            jax.ShapeDtypeStruct(routes.shape, jnp.int32),
-        ),
-        in_specs=[VMEM] * 11 + [ANY] + [VMEM] * 3,
-        out_specs=(VMEM, VMEM, VMEM),
+        functools.partial(front_kernel, size, pair, tp_size),
+        out_shape=jax.ShapeDtypeStruct((chunks, out_rows, model_width // chunks), jnp.bfloat16),
+        in_specs=[VMEM] * 10 + [ANY] + [VMEM] * 3,
+        out_specs=VMEM,
         scratch_shapes=[
             pltpu.VMEM((size, 2, rows, HEAD), jnp.bfloat16),
             pltpu.VMEM((size, rows // HEAD, HEAD), jnp.int32),
@@ -453,7 +408,6 @@
         key_gain[None, :],
         row_table,
         col_table,
-        routes.T,
         out_gain[None, :],
         out_proj,
         residual,
@@ -463,158 +417,479 @@
 
 
 def expert_kernel(
-    outer_size,
-    inner_size,
+    steps,
+    plane,
     tp_size,
     x_ref,
-    gate_ref,
-    up_ref,
-    down_ref,
+    route_ref,
+    weight_ref,
+    gate_hbm,
+    up_hbm,
+    down_hbm,
+    gain_ref,
+    bias_ref,
     o_ref,
+    xs,
+    routes,
+    weights,
+    slots,
+    outb,
     held,
     served,
+    back,
+    given,
+    brought,
+    own_sum,
+    gate_acc,
+    up_acc,
+    gate_w,
+    up_w,
+    down_w,
+    line_send,
+    line_recv,
     out_send,
     out_recv,
     back_send,
     back_recv,
+    sum_send,
+    sum_recv,
     own_sem,
 ):
     me = lax.axis_index("sp") * tp_size + lax.axis_index("tp")
-    outer = me // inner_size
-    inner = lax.rem(me, inner_size)
-    size = outer_size * inner_size
-    paired = outer_size & (outer_size - 1) == 0
-    half = outer_size // 2
-    upper, lower = list(range(half, outer_size)), list(range(1, half))
-    if outer_size == 1:
-        send_order, work_order = [0], [0]
-    else:
-        send_order = [group for group in upper + lower if group] + [0]
-        work_order = [0] + [group for group in upper[:1] + lower + upper[1:] if group]
-
-    def mesh_place(index):
+    outer = me // plane
+    inner = lax.rem(me, plane)
+    chunks, rows, width = x_ref.shape
+    block = outb.shape[3]
+    spots = plane * block
+    top = route_ref.shape[0]
+    parts = chunks + 2
+    order = [chunks, chunks + 1] + list(range(chunks))
+
+    loads = [
+        pltpu.make_async_copy(x_ref, xs.at[outer], own_sem.at[0]),
+        pltpu.make_async_copy(route_ref, routes.at[outer], own_sem.at[1]),
+        pltpu.make_async_copy(weight_ref, weights.at[outer], own_sem.at[2]),
+        pltpu.make_async_copy(gate_hbm, gate_w, own_sem.at[3]),
+        pltpu.make_async_copy(up_hbm, up_w, own_sem.at[4]),
+        pltpu.make_async_copy(down_hbm, down_w, own_sem.at[5]),
+    ]
+    for copy in loads:
+        copy.start()
+
+    def device(place, number):
+        index = place * plane + number
         return {"sp": index // tp_size, "tp": lax.rem(index, tp_size)}
 
-    def plane_to(group):
-        if paired:
-            return flipped(outer, group)
-        return lax.rem(outer + group, outer_size)
-
-    def plane_from(group):
-        if paired:
-            return flipped(outer, group)
-        return lax.rem(outer - group + outer_size, outer_size)
-
-    def target_of(group, step):
-        return plane_to(group) * inner_size + lax.rem(inner + step, inner_size)
-
-    def source_of(group, step):
-        return plane_from(group) * inner_size + lax.rem(inner - step + inner_size, inner_size)
-
-    def out_copy(group, step):
-        target = target_of(group, step)
-        return pltpu.make_async_remote_copy(
-            src_ref=x_ref.at[target],
-            dst_ref=held.at[me],
-            send_sem=out_send.at[group * inner_size + step],
-            recv_sem=out_recv.at[group * inner_size + step],
-            device_id=mesh_place(target),
-            device_id_type=pl.DeviceIdType.MESH,
-        )
-
-    def back_copy(group, step):
-        source = source_of(group, step)
-        return pltpu.make_async_remote_copy(
-            src_ref=served.at[source],
-            dst_ref=o_ref.at[me],
-            send_sem=back_send.at[group * inner_size + step],
-            recv_sem=back_recv.at[group * inner_size + step],
-            device_id=mesh_place(source),
-            device_id_type=pl.DeviceIdType.MESH,
-        )
-
-    def each(group, act):
-        def once(step, unused):
-            act(group, step)
-            return unused
-
-        lax.fori_loop(1 if group == 0 else 0, inner_size, once, 0)
-
-    own_out = pltpu.make_async_copy(x_ref.at[me], held.at[me], own_sem.at[0])
-    own_out.start()
+    def on_line(place):
+        return (place >= 0) & (place < steps)
+
     barrier = pltpu.get_barrier_semaphore()
 
-    def greet(group, step):
+    def greet(place, number):
         pl.semaphore_signal(
             barrier,
             inc=1,
-            device_id=mesh_place(target_of(group, step)),
+            device_id=device(place, number),
             device_id_type=pl.DeviceIdType.MESH,
         )
 
-    for group in send_order:
-        each(group, greet)
-    pl.semaphore_wait(barrier, size - 1)
-    for group in send_order:
-        each(group, lambda g, step: out_copy(g, step).start())
-    own_out.wait()
-    local_experts = gate_ref.shape[0]
-    block = held.shape[1]
-    capacity = block // local_experts
-    width = held.shape[2]
-    for group in work_order:
-        each(group, lambda g, step: out_copy(g, step).wait_recv())
-        span = pl.ds(plane_from(group) * inner_size, inner_size)
-        arrived = held[span]
-        for expert in range(local_experts):
-            part = slice(expert * capacity, (expert + 1) * capacity)
-            rows = arrived[:, part].reshape(inner_size * capacity, width)
-            gate = jnp.dot(rows, gate_ref[expert], preferred_element_type=jnp.float32)
-            up = jnp.dot(rows, up_ref[expert], preferred_element_type=jnp.float32)
-            hidden = (gate / (1.0 + jnp.exp(-gate)) * up).astype(jnp.bfloat16)
-            result = jnp.dot(hidden, down_ref[expert], preferred_element_type=jnp.float32)
-            served[span, part] = result.astype(jnp.bfloat16).reshape(inner_size, capacity, width)
-        each(group, lambda g, step: back_copy(g, step).start())
-    own_back = pltpu.make_async_copy(served.at[me], o_ref.at[me], own_sem.at[1])
-    own_back.start()
-    for group in work_order:
-        each(group, lambda g, step: back_copy(g, step).wait_recv())
-    for group in work_order:
-        each(group, lambda g, step: out_copy(g, step).wait_send())
-        each(group, lambda g, step: back_copy(g, step).wait_send())
-    own_back.wait()
-
-
-def run_experts(blocks, gate, up, down, sp_size, tp_size):
-    size = blocks.shape[0]
+    peers = jnp.int32(plane - 1)
+    for sign in (1, -1):
+        there = on_line(outer + sign)
+        pl.when(there)(lambda sign=sign: greet(outer + sign, inner))
+        peers = peers + there.astype(jnp.int32)
+
+    def greet_plane(step, unused):
+        greet(outer, lax.rem(inner + step, plane))
+        return unused
+
+    lax.fori_loop(1, plane, greet_plane, 0)
+    pl.semaphore_wait(barrier, peers)
+
+    def piece(place, part, first):
+        if part == chunks:
+            return (route_ref if first else routes.at[place]), routes.at[place]
+        if part == chunks + 1:
+            return (weight_ref if first else weights.at[place]), weights.at[place]
+        return (x_ref.at[part] if first else xs.at[place, part]), xs.at[place, part]
+
+    def line_copy(way, step, part, first=False):
+        sign = 1 - 2 * way
+        place = outer - sign * (step - 1)
+        src, dst = piece(place, part, first)
+        return pltpu.make_async_remote_copy(
+            src_ref=src,
+            dst_ref=dst,
+            send_sem=line_send.at[way, step, part],
+            recv_sem=line_recv.at[way, step, part],
+            device_id=device(outer + sign, inner),
+            device_id_type=pl.DeviceIdType.MESH,
+        )
+
+    for part in order:
+        for way in range(2):
+            pl.when(on_line(outer + 1 - 2 * way))(
+                lambda way=way, part=part: line_copy(way, 1, part, True).start()
+            )
+
+    def out_copy(source, chunk, target):
+        return pltpu.make_async_remote_copy(
+            src_ref=outb.at[source, chunk, target],
+            dst_ref=held.at[source, chunk, inner],
+            send_sem=out_send.at[source, chunk],
+            recv_sem=out_recv.at[source, chunk],
+            device_id=device(outer, target),
+            device_id_type=pl.DeviceIdType.MESH,
+        )
+
+    def back_copy(source, chunk, target):
+        return pltpu.make_async_remote_copy(
+            src_ref=served.at[source, chunk, target],
+            dst_ref=back.at[source, chunk, inner],
+            send_sem=back_send.at[source, chunk],
+            recv_sem=back_recv.at[source, chunk],
+            device_id=device(outer, target),
+            device_id_type=pl.DeviceIdType.MESH,
+        )
+
+    def others(from_buffer, to_buffer, source, chunk, send_sem, recv_sem):
+        return pltpu.make_async_remote_copy(
+            src_ref=from_buffer.at[source, chunk, pl.ds(0, plane - 1)],
+            dst_ref=to_buffer.at[source, chunk, pl.ds(0, plane - 1)],
+            send_sem=send_sem.at[source, chunk],
+            recv_sem=recv_sem.at[source, chunk],
+            device_id=device(outer, inner),
+            device_id_type=pl.DeviceIdType.MESH,
+        )
+
+    def all_out(source, chunk):
+        return others(outb, held, source, chunk, out_send, out_recv)
+
+    def all_back(source, chunk):
+        return others(served, back, source, chunk, back_send, back_recv)
+
+    def sum_copy(way, dest, chunk):
+        target = outer + 1 - 2 * way
+        slot = jnp.where((dest == target) & (way == 1), steps, dest)
+        return pltpu.make_async_remote_copy(
+            src_ref=given.at[dest, chunk],
+            dst_ref=brought.at[slot, chunk],
+            send_sem=sum_send.at[way, dest, chunk],
+            recv_sem=sum_recv.at[way, dest, chunk],
+            device_id=device(target, inner),
+            device_id_type=pl.DeviceIdType.MESH,
+        )
+
+    def over_ways(step, act):
+        def one(way, unused):
+            source = outer - (1 - 2 * way) * step
+            pl.when(on_line(source) & ((step > 0) | (way == 0)))(lambda: act(way, source))
+            return unused
+
+        lax.fori_loop(0, 2, one, 0)
+
+    def over_chunks(act):
+        def one(chunk, unused):
+            act(chunk)
+            return unused
+
+        lax.fori_loop(0, chunks, one, 0)
+
+    down_iota = lax.broadcasted_iota(jnp.int32, (rows, rows), 0)
+    over_iota = lax.broadcasted_iota(jnp.int32, (rows, rows), 1)
+
+    def place_rows(source):
+        earlier = jnp.where(down_iota < over_iota, 1.0, 0.0).astype(jnp.bfloat16)
+        names = outer * plane + lax.broadcasted_iota(jnp.int32, (plane, rows), 0)
+        start = lax.broadcasted_iota(jnp.int32, (plane, rows), 0).astype(jnp.float32) * block
+        passed = jnp.zeros((plane, 1), jnp.float32)
+        for route in range(top):
+            one_hot = jnp.where(names == routes[source, route : route + 1, :], 1.0, 0.0)
+            before = passed + jnp.dot(
+                one_hot.astype(jnp.bfloat16), earlier, preferred_element_type=jnp.float32
+            )
+            there = jnp.sum(one_hot, axis=0, keepdims=True)
+            slot = jnp.sum((before + start) * one_hot, axis=0, keepdims=True)
+            slots[source, route : route + 1, :] = slot + there - 1.0
+            passed = passed + jnp.sum(one_hot, axis=1, keepdims=True)
+
+    def take_in(step):
+        def small(way, source):
+            def fetch():
+                for part in order[:2]:
+                    wait_part(way, step, part)
+
+            pl.when(step > 0)(fetch)
+            place_rows(source)
+
+        over_ways(step, small)
+
+        def per_chunk(chunk):
+            def forward(way, source):
+                line_dynamic(way, step, chunk).wait_recv()
+                pl.when(on_line(outer + 1 - 2 * way))(
+                    lambda: line_dynamic(way, step + 1, chunk).start()
+                )
+
+            pl.when(step > 0)(lambda: over_ways(step, forward))
+
+            def dispatch(way, source):
+                spot = lax.broadcasted_iota(jnp.int32, (spots, rows), 0).astype(jnp.float32)
+                chosen = spot == slots[source, 0:1, :]
+                for route in range(1, top):
+                    chosen = chosen | (spot == slots[source, route : route + 1, :])
+                select = jnp.where(chosen, 1.0, 0.0).astype(jnp.bfloat16)
+                picked = jnp.dot(select, xs[source, chunk], preferred_element_type=jnp.float32)
+                outb[source, chunk] = picked.astype(jnp.bfloat16).reshape(plane, block, width)
+                held[source, chunk, inner] = outb[source, chunk, inner]
+
+                def give(number, unused):
+                    out_copy(source, chunk, lax.rem(inner + number, plane)).start()
+                    return unused
+
+                lax.fori_loop(1, plane, give, 0)
+
+            over_ways(step, dispatch)
+
+        over_chunks(per_chunk)
+
+    def wait_part(way, step, part):
+        line_copy(way, step, part).wait_recv()
+        pl.when(on_line(outer + 1 - 2 * way))(lambda: line_copy(way, step + 1, part).start())
+
+    def line_dynamic(way, step, chunk):
+        sign = 1 - 2 * way
+        place = outer - sign * (step - 1)
+        return pltpu.make_async_remote_copy(
+            src_ref=xs.at[place, chunk],
+            dst_ref=xs.at[place, chunk],
+            send_sem=line_send.at[way, step, chunk],
+            recv_sem=line_recv.at[way, step, chunk],
+            device_id=device(outer + sign, inner),
+            device_id_type=pl.DeviceIdType.MESH,
+        )
+
+    def serve(step):
+        def run(way, source):
+            gate_acc[...] = jnp.zeros(gate_acc.shape, jnp.float32)
+            up_acc[...] = jnp.zeros(up_acc.shape, jnp.float32)
+
+            def first(chunk):
+                all_out(source, chunk).wait_recv()
+                taken = held[source, chunk].reshape(spots, width)
+                gate_acc[...] += jnp.dot(
+                    taken, gate_w[chunk], preferred_element_type=jnp.float32
+                )
+                up_acc[...] += jnp.dot(taken, up_w[chunk], preferred_element_type=jnp.float32)
+
+            over_chunks(first)
+            gate = gate_acc[...]
+            hidden = (gate / (1.0 + jnp.exp(-gate)) * up_acc[...]).astype(jnp.bfloat16)
+            for chunk in range(chunks):
+                part = slice(chunk * width, (chunk + 1) * width)
+                result = jnp.dot(hidden, down_w[:, part], preferred_element_type=jnp.float32)
+                served[source, chunk] = result.astype(jnp.bfloat16).reshape(plane, block, width)
+                back[source, chunk, inner] = served[source, chunk, inner]
+
+                def give(number, unused, chunk=chunk):
+                    back_copy(source, chunk, lax.rem(inner + number, plane)).start()
+                    return unused
+
+                lax.fori_loop(1, plane, give, 0)
+
+        over_ways(step, run)
+
+    def column(row):
+        return jnp.sum(jnp.where(down_iota == over_iota, row, 0.0), axis=1, keepdims=True)
+
+    def combine(step):
+        def run(way, source):
+            spot = lax.broadcasted_iota(jnp.int32, (rows, spots), 1).astype(jnp.float32)
+            picks, scales = [], []
+            for route in range(top):
+                at = column(slots[source, route : route + 1, :])
+                picks.append(jnp.where(spot == at, 1.0, 0.0).astype(jnp.bfloat16))
+                scales.append(column(weights[source, route : route + 1, :]))
+
+            def one(chunk):
+                all_back(source, chunk).wait_recv()
+                came = back[source, chunk].reshape(spots, width)
+                total = None
+                for pick, scale in zip(picks, scales):
+                    term = jnp.dot(pick, came, preferred_element_type=jnp.float32) * scale
+                    total = term if total is None else total + term
+
+                def keep():
+                    own_sum[chunk] = total
+
+                def hand():
+                    given[source, chunk] = total.astype(jnp.bfloat16)
+                    pl.when(jnp.logical_not(on_line(outer - (1 - 2 * (1 - way)))))(
+                        lambda: sum_copy(1 - way, source, chunk).start()
+                    )
+
+                pl.when(step == 0)(keep)
+                pl.when(step > 0)(hand)
+
+            over_chunks(one)
+
+        over_ways(step, run)
+
+    for copy in loads:
+        copy.wait()
+    take_in(jnp.int32(0))
+    at_end = (outer == 0) | (outer == steps - 1)
+    late = jnp.where(at_end, 2, 1)
+
+    def task(number, unused):
+        step = number // 3
+        kind = lax.rem(number, 3)
+        pl.when(kind == 0)(lambda: serve(step))
+        pl.when((kind == late) & (step + 1 < steps))(lambda: take_in(step + 1))
+        pl.when((kind > 0) & (kind != late))(lambda: combine(step))
+        return unused
+
+    lax.fori_loop(0, 3 * steps, task, 0)
+
+    def pass_sums(turn, unused):
+        def one(chunk):
+            def onward(way, unused):
+                dest = jnp.where(way == 0, turn, steps - 1 - turn)
+                beyond = jnp.where(way == 0, dest > outer, dest < outer)
+
+                def add():
+                    sum_copy(way, dest, chunk).wait_recv()
+                    given[dest, chunk] = (
+                        given[dest, chunk].astype(jnp.float32)
+                        + brought[dest, chunk].astype(jnp.float32)
+                    ).astype(jnp.bfloat16)
+                    sum_copy(way, dest, chunk).start()
+
+                pl.when(beyond & on_line(outer - (1 - 2 * way)))(add)
+                return unused
+
+            lax.fori_loop(0, 2, onward, 0)
+
+        over_chunks(one)
+        return unused
+
+    lax.fori_loop(1, steps, pass_sums, 0)
+
+    def gather(chunk):
+        def from_way(way, unused):
+            def add():
+                sum_copy(way, outer, chunk).wait_recv()
+                slot = jnp.where(way == 0, outer, steps)
+                own_sum[chunk] += brought[slot, chunk].astype(jnp.float32)
+
+            pl.when(on_line(outer - (1 - 2 * way)))(add)
+            return unused
+
+        lax.fori_loop(0, 2, from_way, 0)
+        own_sum[chunk] += alpha_mix * x_ref[chunk].astype(jnp.float32)
+
+    over_chunks(gather)
+    features = chunks * width
+    total = None
+    for chunk in range(chunks):
+        term = jnp.sum(own_sum[chunk], axis=1, keepdims=True)
+        total = term if total is None else total + term
+    center = total / features
+    total = None
+    for chunk in range(chunks):
+        term = jnp.sum(jnp.square(own_sum[chunk] - center), axis=1, keepdims=True)
+        total = term if total is None else total + term
+    spread = lax.rsqrt(total / features + eps_norm)
+    for chunk in range(chunks):
+        part = slice(chunk * width, (chunk + 1) * width)
+        o_ref[:, part] = (
+            (own_sum[chunk] - center) * spread * gain_ref[:, part] + bias_ref[:, part]
+        ).astype(o_ref.dtype)
+
+    def settle(step, unused):
+        def sent(way, source):
+            def onward():
+                for part in range(parts):
+                    line_copy(way, step + 1, part).wait_send()
+
+            pl.when(on_line(outer + 1 - 2 * way))(onward)
+
+            def one(chunk):
+                all_out(source, chunk).wait_send()
+                all_back(source, chunk).wait_send()
+                pl.when(step > 0)(lambda: sum_copy(1 - way, source, chunk).wait_send())
+
+            over_chunks(one)
+
+        def own_up(way, unused):
+            pl.when((step == 0) & (way == 1) & on_line(outer - 1))(own_down)
+            return unused
+
+        def own_down():
+            for part in range(parts):
+                line_copy(1, 1, part).wait_send()
+
+        over_ways(step, sent)
+        own_up(1, 0)
+        return unused
+
+    lax.fori_loop(0, steps, settle, 0)
+
+
+def run_experts(x, routes, route_weights, gate, up, down, gain, bias, sp_size, tp_size):
     pair = 2 if sp_size % 2 == 0 else 1
+    steps, plane = sp_size // pair, pair * tp_size
+    chunks, rows, width = x.shape
+    top = routes.shape[1]
+    hidden = gate.shape[2]
+    spots = plane * (2 * rows * top // (sp_size * tp_size))
+    bf16, f32, dma = jnp.bfloat16, jnp.float32, pltpu.SemaphoreType.DMA
+    blocks = pltpu.VMEM((steps, chunks, plane, spots // plane, width), bf16)
     return pl.pallas_call(
-        functools.partial(expert_kernel, sp_size // pair, pair * tp_size, tp_size),
-        out_shape=jax.ShapeDtypeStruct(blocks.shape, blocks.dtype),
-        in_specs=[VMEM] * 4,
+        functools.partial(expert_kernel, steps, plane, tp_size),
+        out_shape=jax.ShapeDtypeStruct((rows, chunks * width), bf16),
+        in_specs=[VMEM] * 3 + [ANY] * 3 + [VMEM] * 2,
         out_specs=VMEM,
-        scratch_shapes=[pltpu.VMEM(blocks.shape, blocks.dtype) for unused in range(2)]
-        + [pltpu.SemaphoreType.DMA((size,)) for unused in range(4)]
-        + [pltpu.SemaphoreType.DMA((2,))],
+        scratch_shapes=[
+            pltpu.VMEM((steps, chunks, rows, width), bf16),
+            pltpu.VMEM((steps, top, rows), jnp.int32),
+            pltpu.VMEM((steps, top, rows), f32),
+            pltpu.VMEM((steps, top, rows), f32),
+            blocks,
+            blocks,
+            blocks,
+            blocks,
+            pltpu.VMEM((steps, chunks, rows, width), bf16),
+            pltpu.VMEM((steps + 1, chunks, rows, width), bf16),
+            pltpu.VMEM((chunks, rows, width), f32),
+            pltpu.VMEM((spots, hidden), f32),
+            pltpu.VMEM((spots, hidden), f32),
+            pltpu.VMEM((chunks, width, hidden), gate.dtype),
+            pltpu.VMEM((chunks, width, hidden), up.dtype),
+            pltpu.VMEM(down.shape[1:], down.dtype),
+            dma((2, steps + 1, chunks + 2)),
+            dma((2, steps + 1, chunks + 2)),
+            dma((steps, chunks)),
+            dma((steps, chunks)),
+            dma((steps, chunks)),
+            dma((steps, chunks)),
+            dma((2, steps, chunks)),
+            dma((2, steps, chunks)),
+            dma((6,)),
+        ],
         compiler_params=pltpu.CompilerParams(
-            collective_id=2, has_side_effects=True, vmem_limit_bytes=48 * 1024 * 1024
+            collective_id=2, has_side_effects=True, vmem_limit_bytes=60 * 1024 * 1024
         ),
-    )(blocks, gate, up, down)
-
-
-def final_kernel(back_ref, target_ref, weight_ref, mid_ref, gain_ref, bias_ref, o_ref):
-    rows, slots = mid_ref.shape[0], back_ref.shape[0]
-    slot = lax.broadcasted_iota(jnp.int32, (rows, slots), 1)
-    routed = None
-    for route in range(target_ref.shape[1]):
-        select = jnp.where(slot == target_ref[:, route : route + 1], 1.0, 0.0)
-        picked = jnp.dot(
-            select.astype(jnp.bfloat16), back_ref[...], preferred_element_type=jnp.float32
-        )
-        term = picked * weight_ref[:, route : route + 1]
-        routed = term if routed is None else routed + term
-    stream = alpha_mix * mid_ref[...].astype(jnp.float32) + routed
-    o_ref[...] = layer_norm(stream, gain_ref[...], bias_ref[...]).astype(o_ref.dtype)
+    )(
+        x,
+        routes.T,
+        route_weights.T,
+        gate.reshape(chunks, width, hidden),
+        up.reshape(chunks, width, hidden),
+        down.reshape(down.shape[1:]),
+        gain[None, :],
+        bias[None, :],
+    )
 
 
 def per_device(
@@ -641,20 +916,13 @@
     tp_size = lax.axis_size("tp")
     if key_heads.shape[1] != HEAD or expert_gate.shape[0] != 1:
         raise ValueError("unsupported placement")
-    out_rows, model_width = residual.shape
-    local_experts = expert_gate.shape[0]
-    device_total = sp_size * tp_size
-    expert_total = local_experts * device_total
-    capacity = 2 * out_rows * routes.shape[1] // expert_total
-    slots = expert_total * capacity
-    middle, outbound, target_columns = run_front(
+    middle = run_front(
         queries,
         key_heads,
         value_heads,
         documents,
         query_gain,
         key_gain,
-        routes,
         out_gain,
         out_proj,
         residual,
@@ -662,29 +930,19 @@
         mid_bias,
         sp_size,
         tp_size,
-        capacity,
+        CHUNKS,
     )
-    returned = run_experts(
-        outbound.reshape(device_total, local_experts * capacity, model_width),
+    return run_experts(
+        middle,
+        routes,
+        route_weights,
         expert_gate,
         expert_up,
         expert_down,
+        final_gain,
+        final_bias,
         sp_size,
         tp_size,
-    )
-    return pl.pallas_call(
-        final_kernel,
-        out_shape=jax.ShapeDtypeStruct((out_rows, model_width), jnp.bfloat16),
-        in_specs=[VMEM] * 6,
-        out_specs=VMEM,
-        compiler_params=pltpu.CompilerParams(vmem_limit_bytes=48 * 1024 * 1024),
-    )(
-        returned.reshape(slots, model_width),
-        target_columns,
-        route_weights,
-        middle,
-        final_gain[None, :],
-        final_bias[None, :],
     )
 
 

time: 158 us -> 168 us (1.063)
  the two profiles are of different devices: /device:TPU:9 before, /device:TPU:0 now
where the time goes in v2:
time: 168 us
  Pallas kernels  162 us (96%)
  local copies, waits for them, and re-layouts  3.4 us (2%)
  other arithmetic  1.71 us (1%)
    pallas_call x1, Pallas kernels, run_experts(): pl.pallas_call(functools.partial(expert_kernel, steps, plane, tp_size), o...  113 us
    pallas_call x1, Pallas kernels, run_front(): pl.pallas_call(functools.partial(front_kernel, size, pair, tp_size), out_...  49 us

profile of v2, /device:TPU:0, one launch (start us, length us, event | category | flops | bytes accessed | tf_op | source)
XLA Modules:
  0.0 167.6 jit_solution(17118622297412058530)
XLA Ops:
  0.0 0.1 multiply_cosine_fusion.1
  0.1 0.1 fusion.7
  0.2 0.6 pad_maximum_fusion.5.row_ref
  0.8 0.2 multiply_cosine_fusion
  1.0 0.1 fusion.1
  1.1 0.6 pad_maximum_fusion.col_ref
  1.8 1.5 broadcast_in_dim.37.qdoc_ref
  3.3 49.0 %shard_map.172.x_ref = bf16[4,128,512]{2,1,0:T(8,128)(2,1)} custom-call(bf16[512,256]{1,0:T(8,128)(2,1)} %q_ref.1, bf16[512,128]{1,0:T(8,128)(2,1)} %k_ref.1, bf16[512,128]{1,0:T(8,128)(2,1)} %v_ref.1, s32[4,128]{1,0:T(4,128)} %bitcast.26, s32[512,128]{1,0:T(8,128)} %broadcast_in_dim.37.qdoc_ref, f32[1,128]{1,0:T(1,128)} %bitcast.32, f32[1,128]{1,0:T(1,128)} %bitcast.33, ...), custom_call_target="tpu_custom_call" | custom-call | tf_op jit(solution)/shard_map/pallas_call | solution.py:375
  52.3 113.4 %shard_map.173 = bf16[128,2048]{1,0:T(8,128)(2,1)} custom-call(bf16[4,128,512]{2,1,0:T(8,128)(2,1)} %shard_map.172.x_ref, s32[2,128]{1,0:T(2,128)} %bitcast.30, f32[2,128]{1,0:T(2,128)} %bitcast.31, bf16[4,512,512]{2,1,0:T(8,128)(2,1)} %bitcast.21, bf16[4,512,512]{2,1,0:T(8,128)(2,1)} %bitcast.22, bf16[512,2048]{1,0:T(8,128)(2,1)} %bitcast.23, ...), custom_call_target="tpu_custom_call" | custom-call | tf_op jit(solution)/shard_map/pallas_call | solution.py:848
  165.7 1.9 %copy.20 = bf16[128,2048]{1,0:T(8,128)(2,1)} copy(bf16[128,2048]{1,0:T(8,128)(2,1)} %shard_map.173) | data formatting | bytes 1048576
  (5 shorter events, 0.0 us)

commit v3 on v2

--- a/solution.py
+++ b/solution.py
@@ -10,6 +10,8 @@
 HEAD = 128
 GRID = 64
 CHUNKS = 4
+SERVE_LAG = 3
+COMBINE_LAG = 2
 
 
 eps_norm = 1e-06
@@ -442,6 +444,8 @@
     own_sum,
     gate_acc,
     up_acc,
+    picks,
+    scales,
     gate_w,
     up_w,
     down_w,
@@ -526,11 +530,17 @@
             device_id_type=pl.DeviceIdType.MESH,
         )
 
-    for part in order:
-        for way in range(2):
-            pl.when(on_line(outer + 1 - 2 * way))(
-                lambda way=way, part=part: line_copy(way, 1, part, True).start()
-            )
+    half = chunks // 2
+    depth = (outer, steps - 1 - outer)
+
+    def send_own(way, send):
+        there = on_line(outer + 1 - 2 * way)
+        for part in send:
+            pl.when(there)(lambda part=part: line_copy(way, 1, part, True).start())
+
+    for way in range(2):
+        send_own(way, order[: 2 + half])
+        pl.when(depth[way] == 0)(lambda way=way: send_own(way, order[2 + half :]))
 
     def out_copy(source, chunk, target):
         return pltpu.make_async_remote_copy(
@@ -613,45 +623,42 @@
             slots[source, route : route + 1, :] = slot + there - 1.0
             passed = passed + jnp.sum(one_hot, axis=1, keepdims=True)
 
-    def take_in(step):
-        def small(way, source):
-            def fetch():
-                for part in order[:2]:
-                    wait_part(way, step, part)
-
-            pl.when(step > 0)(fetch)
-            place_rows(source)
-
-        over_ways(step, small)
-
-        def per_chunk(chunk):
-            def forward(way, source):
-                line_dynamic(way, step, chunk).wait_recv()
-                pl.when(on_line(outer + 1 - 2 * way))(
-                    lambda: line_dynamic(way, step + 1, chunk).start()
-                )
-
-            pl.when(step > 0)(lambda: over_ways(step, forward))
-
-            def dispatch(way, source):
-                spot = lax.broadcasted_iota(jnp.int32, (spots, rows), 0).astype(jnp.float32)
-                chosen = spot == slots[source, 0:1, :]
-                for route in range(1, top):
-                    chosen = chosen | (spot == slots[source, route : route + 1, :])
-                select = jnp.where(chosen, 1.0, 0.0).astype(jnp.bfloat16)
-                picked = jnp.dot(select, xs[source, chunk], preferred_element_type=jnp.float32)
-                outb[source, chunk] = picked.astype(jnp.bfloat16).reshape(plane, block, width)
-                held[source, chunk, inner] = outb[source, chunk, inner]
-
-                def give(number, unused):
-                    out_copy(source, chunk, lax.rem(inner + number, plane)).start()
-                    return unused
-
-                lax.fori_loop(1, plane, give, 0)
-
-            over_ways(step, dispatch)
-
-        over_chunks(per_chunk)
+    def dispatch(source, chunk):
+        pl.when(chunk == 0)(lambda: place_rows(source))
+        spot = lax.broadcasted_iota(jnp.int32, (spots, rows), 0).astype(jnp.float32)
+        chosen = spot == slots[source, 0:1, :]
+        for route in range(1, top):
+            chosen = chosen | (spot == slots[source, route : route + 1, :])
+        select = jnp.where(chosen, 1.0, 0.0).astype(jnp.bfloat16)
+        picked = jnp.dot(select, xs[source, chunk], preferred_element_type=jnp.float32)
+        outb[source, chunk] = picked.astype(jnp.bfloat16).reshape(plane, block, width)
+        held[source, chunk, inner] = outb[source, chunk, inner]
+
+        def give(number, unused):
+            out_copy(source, chunk, lax.rem(inner + number, plane)).start()
+            return unused
+
+        lax.fori_loop(1, plane, give, 0)
+
+    def place_of(way, number, full):
+        pairs = number // half
+        out = pairs < full
+        step = jnp.where(out, pairs + 1, 2 * full - pairs)
+        chunk = jnp.where(out, 0, half) + lax.rem(number, half)
+        return step, chunk, outer - (1 - 2 * way) * step
+
+    def receive(way, number, full):
+        step, chunk, source = place_of(way, number, full)
+
+        def small():
+            for part in order[:2]:
+                wait_part(way, step, part)
+
+        pl.when(chunk == 0)(small)
+        line_dynamic(way, step, chunk).wait_recv()
+        pl.when(on_line(outer + 1 - 2 * way))(
+            lambda: line_dynamic(way, step + 1, chunk).start()
+        )
 
     def wait_part(way, step, part):
         line_copy(way, step, part).wait_recv()
@@ -669,111 +676,162 @@
             device_id_type=pl.DeviceIdType.MESH,
         )
 
-    def serve(step):
-        def run(way, source):
-            gate_acc[...] = jnp.zeros(gate_acc.shape, jnp.float32)
-            up_acc[...] = jnp.zeros(up_acc.shape, jnp.float32)
-
-            def first(chunk):
-                all_out(source, chunk).wait_recv()
-                taken = held[source, chunk].reshape(spots, width)
-                gate_acc[...] += jnp.dot(
-                    taken, gate_w[chunk], preferred_element_type=jnp.float32
-                )
-                up_acc[...] += jnp.dot(taken, up_w[chunk], preferred_element_type=jnp.float32)
-
-            over_chunks(first)
-            gate = gate_acc[...]
-            hidden = (gate / (1.0 + jnp.exp(-gate)) * up_acc[...]).astype(jnp.bfloat16)
-            for chunk in range(chunks):
-                part = slice(chunk * width, (chunk + 1) * width)
-                result = jnp.dot(hidden, down_w[:, part], preferred_element_type=jnp.float32)
-                served[source, chunk] = result.astype(jnp.bfloat16).reshape(plane, block, width)
-                back[source, chunk, inner] = served[source, chunk, inner]
-
-                def give(number, unused, chunk=chunk):
-                    back_copy(source, chunk, lax.rem(inner + number, plane)).start()
-                    return unused
-
-                lax.fori_loop(1, plane, give, 0)
-
-        over_ways(step, run)
+    def serve(source, chunk):
+        all_out(source, chunk).wait_recv()
+        taken = held[source, chunk].reshape(spots, width)
+        gate = jnp.dot(taken, gate_w[chunk], preferred_element_type=jnp.float32)
+        up = jnp.dot(taken, up_w[chunk], preferred_element_type=jnp.float32)
+
+        def fresh():
+            gate_acc[source] = gate
+            up_acc[source] = up
+
+        def add():
+            gate_acc[source] += gate
+            up_acc[source] += up
+
+        pl.when(chunk == 0)(fresh)
+        pl.when(chunk > 0)(add)
+        pl.when(chunk == chunks - 1)(lambda: finish(source))
+
+    def finish(source):
+        gate = gate_acc[source]
+        hidden = (gate / (1.0 + jnp.exp(-gate)) * up_acc[source]).astype(jnp.bfloat16)
+        for chunk in range(chunks):
+            part = slice(chunk * width, (chunk + 1) * width)
+            result = jnp.dot(hidden, down_w[:, part], preferred_element_type=jnp.float32)
+            served[source, chunk] = result.astype(jnp.bfloat16).reshape(plane, block, width)
+            back[source, chunk, inner] = served[source, chunk, inner]
+
+            def give(number, unused, chunk=chunk):
+                back_copy(source, chunk, lax.rem(inner + number, plane)).start()
+                return unused
+
+            lax.fori_loop(1, plane, give, 0)
 
     def column(row):
         return jnp.sum(jnp.where(down_iota == over_iota, row, 0.0), axis=1, keepdims=True)
 
-    def combine(step):
-        def run(way, source):
+    def combine(way, source, chunk):
+        def prepare():
             spot = lax.broadcasted_iota(jnp.int32, (rows, spots), 1).astype(jnp.float32)
-            picks, scales = [], []
             for route in range(top):
                 at = column(slots[source, route : route + 1, :])
-                picks.append(jnp.where(spot == at, 1.0, 0.0).astype(jnp.bfloat16))
-                scales.append(column(weights[source, route : route + 1, :]))
-
-            def one(chunk):
-                all_back(source, chunk).wait_recv()
-                came = back[source, chunk].reshape(spots, width)
-                total = None
-                for pick, scale in zip(picks, scales):
-                    term = jnp.dot(pick, came, preferred_element_type=jnp.float32) * scale
-                    total = term if total is None else total + term
-
-                def keep():
-                    own_sum[chunk] = total
-
-                def hand():
-                    given[source, chunk] = total.astype(jnp.bfloat16)
-                    pl.when(jnp.logical_not(on_line(outer - (1 - 2 * (1 - way)))))(
-                        lambda: sum_copy(1 - way, source, chunk).start()
-                    )
-
-                pl.when(step == 0)(keep)
-                pl.when(step > 0)(hand)
-
-            over_chunks(one)
-
-        over_ways(step, run)
-
-    for copy in loads:
+                picks[way, route] = jnp.where(spot == at, 1.0, 0.0).astype(jnp.bfloat16)
+                scale = column(weights[source, route : route + 1, :])
+                scales[way, route] = jnp.broadcast_to(scale, scales.shape[2:])
+
+        pl.when(chunk == 0)(prepare)
+        all_back(source, chunk).wait_recv()
+        came = back[source, chunk].reshape(spots, width)
+        total = None
+        for route in range(top):
+            term = jnp.dot(picks[way, route], came, preferred_element_type=jnp.float32)
+            term = term * scales[way, route][:, 0:1]
+            total = term if total is None else total + term
+
+        def keep():
+            own_sum[chunk] = total
+
+        def hand():
+            given[source, chunk] = total.astype(jnp.bfloat16)
+            pl.when(jnp.logical_not(on_line(outer - (1 - 2 * (1 - way)))))(
+                lambda: sum_copy(1 - way, source, chunk).start()
+            )
+
+        pl.when(way == 2)(keep)
+        pl.when(way < 2)(hand)
+
+    for copy in loads[:3]:
         copy.wait()
-    take_in(jnp.int32(0))
-    at_end = (outer == 0) | (outer == steps - 1)
-    late = jnp.where(at_end, 2, 1)
-
-    def task(number, unused):
-        step = number // 3
-        kind = lax.rem(number, 3)
-        pl.when(kind == 0)(lambda: serve(step))
-        pl.when((kind == late) & (step + 1 < steps))(lambda: take_in(step + 1))
-        pl.when((kind > 0) & (kind != late))(lambda: combine(step))
+
+    def first(chunk, unused):
+        dispatch(outer, chunk)
         return unused
 
-    lax.fori_loop(0, 3 * steps, task, 0)
-
-    def pass_sums(turn, unused):
-        def one(chunk):
-            def onward(way, unused):
-                dest = jnp.where(way == 0, turn, steps - 1 - turn)
-                beyond = jnp.where(way == 0, dest > outer, dest < outer)
-
-                def add():
-                    sum_copy(way, dest, chunk).wait_recv()
-                    given[dest, chunk] = (
-                        given[dest, chunk].astype(jnp.float32)
-                        + brought[dest, chunk].astype(jnp.float32)
-                    ).astype(jnp.bfloat16)
-                    sum_copy(way, dest, chunk).start()
-
-                pl.when(beyond & on_line(outer - (1 - 2 * way)))(add)
-                return unused
-
-            lax.fori_loop(0, 2, onward, 0)
-
-        over_chunks(one)
+    lax.fori_loop(0, chunks, first, 0)
+
+    def stage(number, unused):
+        def load_weights():
+            for copy in loads[3:]:
+                copy.wait()
+
+        def each_way(way, unused):
+            full = jnp.where(way == 0, depth[0], depth[1])
+
+            def take():
+                receive(way, number, full)
+
+                def rest():
+                    for part in order[2 + half :]:
+                        line_copy(way, 1, part, True).start()
+
+                pl.when((number == full * chunks - 1) & on_line(outer + 1 - 2 * way))(rest)
+                step, chunk, source = place_of(way, number, full)
+                dispatch(source, chunk)
+
+            pl.when(number < full * chunks)(take)
+            return unused
+
+        lax.fori_loop(0, 2, each_way, 0)
+        pl.when(number == 0)(load_weights)
+
+        def serve_way(way, unused):
+            full = jnp.where(way == 0, depth[0], depth[1])
+            at = number - SERVE_LAG
+            step, chunk, source = place_of(way, at, full)
+            mine = way == 2
+            source = jnp.where(mine, outer, source)
+            chunk = jnp.where(mine, number, chunk)
+            live = jnp.where(mine, number < chunks, (at >= 0) & (at < full * chunks))
+            pl.when(live)(lambda: serve(source, chunk))
+            return unused
+
+        lax.fori_loop(0, 3, serve_way, 0)
+
+        def combine_way(turn, unused):
+            way = turn // 2
+            full = jnp.where(way == 0, depth[0], depth[1])
+            start = (full + 1) * half - 1 + SERVE_LAG + COMBINE_LAG
+            at = 2 * (number - start) + lax.rem(turn, 2)
+            mine = way == 2
+            at = jnp.where(mine, 2 * (number - (chunks + COMBINE_LAG)) + lax.rem(turn, 2), at)
+            source = jnp.where(mine, outer, outer - (1 - 2 * way) * (full - at // chunks))
+            limit = jnp.where(mine, chunks, full * chunks)
+            live = (at >= 0) & (at < limit)
+            pl.when(live)(lambda: combine(way, source, lax.rem(at, chunks)))
+            return unused
+
+        lax.fori_loop(0, 6, combine_way, 0)
         return unused
 
-    lax.fori_loop(1, steps, pass_sums, 0)
+    last = chunks * (steps - 1) + SERVE_LAG + COMBINE_LAG + chunks
+    lax.fori_loop(0, last, stage, 0)
+
+    ahead = 2 * (2 * outer - (steps - 1))
+    delays = (jnp.maximum(ahead, 0), jnp.maximum(-ahead, 0))
+
+    def pass_sums(number, unused):
+        for way in range(2):
+            at = number - delays[way]
+            turn = at // chunks
+            chunk = lax.rem(at, chunks)
+            dest = steps - 1 - turn if way == 0 else turn
+            beyond = (dest > outer) if way == 0 else (dest < outer)
+            live = (at >= 0) & (turn < steps - 1) & beyond & on_line(outer - (1 - 2 * way))
+
+            def add(way=way, dest=dest, chunk=chunk):
+                sum_copy(way, dest, chunk).wait_recv()
+                given[dest, chunk] = (
+                    given[dest, chunk].astype(jnp.float32)
+                    + brought[dest, chunk].astype(jnp.float32)
+                ).astype(jnp.bfloat16)
+                sum_copy(way, dest, chunk).start()
+
+            pl.when(live)(add)
+        return unused
+
+    lax.fori_loop(0, (steps - 1) * chunks + 2 * (steps - 1), pass_sums, 0)
 
     def gather(chunk):
         def from_way(way, unused):
@@ -862,8 +920,10 @@
             pltpu.VMEM((steps, chunks, rows, width), bf16),
             pltpu.VMEM((steps + 1, chunks, rows, width), bf16),
             pltpu.VMEM((chunks, rows, width), f32),
-            pltpu.VMEM((spots, hidden), f32),
-            pltpu.VMEM((spots, hidden), f32),
+            pltpu.VMEM((steps, spots, hidden), f32),
+            pltpu.VMEM((steps, spots, hidden), f32),
+            pltpu.VMEM((3, top, rows, spots), bf16),
+            pltpu.VMEM((3, top, rows, HEAD), f32),
             pltpu.VMEM((chunks, width, hidden), gate.dtype),
             pltpu.VMEM((chunks, width, hidden), up.dtype),
             pltpu.VMEM(down.shape[1:], down.dtype),

time: 168 us -> 135 us (0.80)
  the two profiles are of different devices: /device:TPU:0 before, /device:TPU:9 now
where the time goes in v3:
time: 135 us
  Pallas kernels  130 us (96%)
  local copies, waits for them, and re-layouts  3.4 us (3%)
  other arithmetic  1.71 us (1%)
    pallas_call x1, Pallas kernels, run_experts(): pl.pallas_call(functools.partial(expert_kernel, steps, plane, tp_size), o...  85.9 us
    pallas_call x1, Pallas kernels, run_front(): pl.pallas_call(functools.partial(front_kernel, size, pair, tp_size), out_...  43.8 us

profile of v3, /device:TPU:9, one launch (start us, length us, event | category | flops | bytes accessed | tf_op | source)
XLA Modules:
  0.0 134.9 jit_solution(14819265778416616295)
XLA Ops:
  0.0 0.1 multiply_cosine_fusion.1
  0.1 0.1 fusion.7
  0.2 0.6 pad_maximum_fusion.5.row_ref
  0.8 0.2 multiply_cosine_fusion
  1.0 0.1 fusion.1
  1.1 0.6 pad_maximum_fusion.col_ref
  1.8 1.5 %broadcast_in_dim.37.qdoc_ref = s32[512,128]{1,0:T(8,128)} broadcast(s32[512]{0:T(512)} %param.21), dimensions={0} | broadcast | bytes 264192 | tf_op jit(solution)/shard_map/broadcast_in_dim | solution.py:375
  3.3 43.8 %shard_map.172.x_ref = bf16[4,128,512]{2,1,0:T(8,128)(2,1)} custom-call(bf16[512,256]{1,0:T(8,128)(2,1)} %q_ref.1, bf16[512,128]{1,0:T(8,128)(2,1)} %k_ref.1, bf16[512,128]{1,0:T(8,128)(2,1)} %v_ref.1, s32[4,128]{1,0:T(4,128)} %bitcast.26, s32[512,128]{1,0:T(8,128)} %broadcast_in_dim.37.qdoc_ref, f32[1,128]{1,0:T(1,128)} %bitcast.32, f32[1,128]{1,0:T(1,128)} %bitcast.33, ...), custom_call_target="tpu_custom_call" | custom-call | tf_op jit(solution)/shard_map/pallas_call | solution.py:377
  47.1 85.9 %shard_map.173 = bf16[128,2048]{1,0:T(8,128)(2,1)} custom-call(bf16[4,128,512]{2,1,0:T(8,128)(2,1)} %shard_map.172.x_ref, s32[2,128]{1,0:T(2,128)} %bitcast.30, f32[2,128]{1,0:T(2,128)} %bitcast.31, bf16[4,512,512]{2,1,0:T(8,128)(2,1)} %bitcast.21, bf16[4,512,512]{2,1,0:T(8,128)(2,1)} %bitcast.22, bf16[512,2048]{1,0:T(8,128)(2,1)} %bitcast.23, ...), custom_call_target="tpu_custom_call" | custom-call | tf_op jit(solution)/shard_map/pallas_call | solution.py:906
  133.0 1.9 %copy.20 = bf16[128,2048]{1,0:T(8,128)(2,1)} copy(bf16[128,2048]{1,0:T(8,128)(2,1)} %shard_map.173) | data formatting | bytes 1048576
  (5 shorter events, 0.0 us)

commit v4 on v3

--- a/solution.py
+++ b/solution.py
@@ -12,6 +12,10 @@
 CHUNKS = 4
 SERVE_LAG = 3
 COMBINE_LAG = 2
+EDGE_SERVE_LAG = 2
+EDGE_COMBINE_LAG = 2
+PASS_LAG = 2
+PASS_GAP = 2
 
 
 eps_norm = 1e-06
@@ -43,11 +47,9 @@
     k_ref,
     v_ref,
     doc_ref,
-    qdoc_ref,
     q_gain_ref,
     k_gain_ref,
-    row_ref,
-    col_ref,
+    freq_ref,
     gain_ref,
     proj_hbm,
     res_ref,
@@ -56,6 +58,9 @@
     mid_ref,
     kv,
     docs,
+    qdoc_ref,
+    row_ref,
+    col_ref,
     q_rot,
     m_ref,
     l_ref,
@@ -154,6 +159,15 @@
 
     send_own(1)
     send_own(2)
+    lanes = lax.broadcasted_iota(jnp.int32, (1, HEAD), 1)
+    along = lax.rem(lanes, HEAD // 2) < HEAD // 4
+    side = jnp.where(lanes < HEAD // 2, -1.0, 1.0)
+    first_row = (me * (rows // GRID)).astype(jnp.float32)
+    for table, start, mask in ((row_ref, first_row, along), (col_ref, 0.0, ~along)):
+        numbers = lax.broadcasted_iota(jnp.int32, table.shape[1:], 0).astype(jnp.float32)
+        angles = (numbers + start) * freq_ref[...]
+        table[0] = jnp.where(mask, jnp.cos(angles), 0.0)
+        table[1] = jnp.where(mask, jnp.sin(angles) * side, 0.0)
     grid_rows = row_ref.shape[1]
     span = col_ref.shape[1]
 
@@ -184,6 +198,14 @@
         return unused
 
     lax.fori_loop(0, grid_rows, turn_queries, 0)
+    down = lax.broadcasted_iota(jnp.int32, (HEAD, HEAD), 0)
+    over = lax.broadcasted_iota(jnp.int32, (HEAD, HEAD), 1)
+    for number in range(pieces):
+        named = doc_ref[number : number + 1].astype(jnp.float32)
+        column = jnp.sum(jnp.where(down == over, named, 0.0), axis=1, keepdims=True)
+        qdoc_ref[number * HEAD : (number + 1) * HEAD] = jnp.broadcast_to(
+            column, (HEAD, HEAD)
+        ).astype(jnp.int32)
     m_ref[...] = jnp.full(m_ref.shape, -1e30, jnp.float32)
     l_ref[...] = jnp.zeros(l_ref.shape, jnp.float32)
     acc_ref[...] = jnp.zeros(acc_ref.shape, jnp.float32)
@@ -220,7 +242,7 @@
                 )
                 m_ref[head, part] = new_max
 
-    def stage(step, unused):
+    def receive(step):
         for group in ((1, 2), (0,)):
             for way in range(2):
                 sign = 1 - 2 * way
@@ -240,6 +262,7 @@
 
                 pl.when((step > 0) & on_line(outer - sign * step))(take)
 
+    def stage(step, unused):
         def visit(number, unused):
             way = lax.rem(number, 2)
             across = number // 2
@@ -258,7 +281,9 @@
             pl.when(on_line(there) & ((step > 0) | (way == 0)))(work)
             return unused
 
-        lax.fori_loop(0, 2 * pair, visit, 0)
+        lax.fori_loop(0, 2, visit, 0)
+        pl.when(step + 1 < steps)(lambda: receive(step + 1))
+        lax.fori_loop(2, 2 * pair, visit, 0)
         return unused
 
     lax.fori_loop(0, steps, stage, 0)
@@ -326,28 +351,6 @@
         return unused
 
     lax.fori_loop(0, steps, settle, 0)
-
-
-def trig_tables(tok_rows, offset):
-    pair_count = HEAD // 4
-    inv_freq = theta_base ** (-jnp.arange(pair_count, dtype=jnp.float32) / pair_count)
-    grid_rows = (offset // GRID + jnp.arange(tok_rows // GRID, dtype=jnp.int32)).astype(jnp.float32)
-    grid_cols = jnp.arange(GRID, dtype=jnp.int32).astype(jnp.float32)
-    tables = []
-    for at, place in enumerate((grid_rows, grid_cols)):
-        angles = place[:, None] * inv_freq[None, :]
-        blank = jnp.zeros_like(angles)
-        cosine, sine = jnp.cos(angles), jnp.sin(angles)
-        order = (lambda a, b: [a, blank, b, blank]) if at == 0 else (lambda a, b: [blank, a, blank, b])
-        tables.append(
-            jnp.stack(
-                [
-                    jnp.concatenate(order(cosine, cosine), axis=1),
-                    jnp.concatenate(order(-sine, sine), axis=1),
-                ]
-            )
-        )
-    return tables
 
 
 def run_front(
@@ -371,17 +374,20 @@
     grouped = width // HEAD
     out_rows, model_width = residual.shape
     steps = size // pair
-    row_table, col_table = trig_tables(rows, lax.axis_index("sp") * rows)
-    query_docs = jnp.broadcast_to(documents[:, None], (rows, HEAD))
+    pair_count = HEAD // 4
+    inv_freq = theta_base ** (-jnp.arange(pair_count, dtype=jnp.float32) / pair_count)
     dma = pltpu.SemaphoreType.DMA
     return pl.pallas_call(
         functools.partial(front_kernel, size, pair, tp_size),
         out_shape=jax.ShapeDtypeStruct((chunks, out_rows, model_width // chunks), jnp.bfloat16),
-        in_specs=[VMEM] * 10 + [ANY] + [VMEM] * 3,
+        in_specs=[VMEM] * 8 + [ANY] + [VMEM] * 3,
         out_specs=VMEM,
         scratch_shapes=[
             pltpu.VMEM((size, 2, rows, HEAD), jnp.bfloat16),
             pltpu.VMEM((size, rows // HEAD, HEAD), jnp.int32),
+            pltpu.VMEM((rows, HEAD), jnp.int32),
+            pltpu.VMEM((2, rows // GRID, HEAD), jnp.float32),
+            pltpu.VMEM((2, GRID, HEAD), jnp.float32),
             pltpu.VMEM((grouped, rows, HEAD), jnp.bfloat16),
             pltpu.VMEM((grouped, rows, HEAD), jnp.float32),
             pltpu.VMEM((grouped, rows, HEAD), jnp.float32),
@@ -405,11 +411,9 @@
         keys,
         values,
         documents.reshape(rows // HEAD, HEAD),
-        query_docs,
         query_gain[None, :],
         key_gain[None, :],
-        row_table,
-        col_table,
+        jnp.tile(inv_freq, 4)[None, :],
         out_gain[None, :],
         out_proj,
         residual,
@@ -444,6 +448,7 @@
     own_sum,
     gate_acc,
     up_acc,
+    selects,
     picks,
     scales,
     gate_w,
@@ -622,15 +627,15 @@
             slot = jnp.sum((before + start) * one_hot, axis=0, keepdims=True)
             slots[source, route : route + 1, :] = slot + there - 1.0
             passed = passed + jnp.sum(one_hot, axis=1, keepdims=True)
-
-    def dispatch(source, chunk):
-        pl.when(chunk == 0)(lambda: place_rows(source))
         spot = lax.broadcasted_iota(jnp.int32, (spots, rows), 0).astype(jnp.float32)
         chosen = spot == slots[source, 0:1, :]
         for route in range(1, top):
             chosen = chosen | (spot == slots[source, route : route + 1, :])
-        select = jnp.where(chosen, 1.0, 0.0).astype(jnp.bfloat16)
-        picked = jnp.dot(select, xs[source, chunk], preferred_element_type=jnp.float32)
+        selects[source] = jnp.where(chosen, 1.0, 0.0).astype(jnp.bfloat16)
+
+    def dispatch(source, chunk):
+        pl.when(chunk == 0)(lambda: place_rows(source))
+        picked = jnp.dot(selects[source], xs[source, chunk], preferred_element_type=jnp.float32)
         outb[source, chunk] = picked.astype(jnp.bfloat16).reshape(plane, block, width)
         held[source, chunk, inner] = outb[source, chunk, inner]
 
@@ -724,10 +729,11 @@
         pl.when(chunk == 0)(prepare)
         all_back(source, chunk).wait_recv()
         came = back[source, chunk].reshape(spots, width)
+        chosen = picks[way].reshape(top * rows, spots)
+        picked = jnp.dot(chosen, came, preferred_element_type=jnp.float32)
         total = None
         for route in range(top):
-            term = jnp.dot(picks[way, route], came, preferred_element_type=jnp.float32)
-            term = term * scales[way, route][:, 0:1]
+            term = picked[route * rows : (route + 1) * rows] * scales[way, route][:, 0:1]
             total = term if total is None else total + term
 
         def keep():
@@ -741,72 +747,6 @@
 
         pl.when(way == 2)(keep)
         pl.when(way < 2)(hand)
-
-    for copy in loads[:3]:
-        copy.wait()
-
-    def first(chunk, unused):
-        dispatch(outer, chunk)
-        return unused
-
-    lax.fori_loop(0, chunks, first, 0)
-
-    def stage(number, unused):
-        def load_weights():
-            for copy in loads[3:]:
-                copy.wait()
-
-        def each_way(way, unused):
-            full = jnp.where(way == 0, depth[0], depth[1])
-
-            def take():
-                receive(way, number, full)
-
-                def rest():
-                    for part in order[2 + half :]:
-                        line_copy(way, 1, part, True).start()
-
-                pl.when((number == full * chunks - 1) & on_line(outer + 1 - 2 * way))(rest)
-                step, chunk, source = place_of(way, number, full)
-                dispatch(source, chunk)
-
-            pl.when(number < full * chunks)(take)
-            return unused
-
-        lax.fori_loop(0, 2, each_way, 0)
-        pl.when(number == 0)(load_weights)
-
-        def serve_way(way, unused):
-            full = jnp.where(way == 0, depth[0], depth[1])
-            at = number - SERVE_LAG
-            step, chunk, source = place_of(way, at, full)
-            mine = way == 2
-            source = jnp.where(mine, outer, source)
-            chunk = jnp.where(mine, number, chunk)
-            live = jnp.where(mine, number < chunks, (at >= 0) & (at < full * chunks))
-            pl.when(live)(lambda: serve(source, chunk))
-            return unused
-
-        lax.fori_loop(0, 3, serve_way, 0)
-
-        def combine_way(turn, unused):
-            way = turn // 2
-            full = jnp.where(way == 0, depth[0], depth[1])
-            start = (full + 1) * half - 1 + SERVE_LAG + COMBINE_LAG
-            at = 2 * (number - start) + lax.rem(turn, 2)
-            mine = way == 2
-            at = jnp.where(mine, 2 * (number - (chunks + COMBINE_LAG)) + lax.rem(turn, 2), at)
-            source = jnp.where(mine, outer, outer - (1 - 2 * way) * (full - at // chunks))
-            limit = jnp.where(mine, chunks, full * chunks)
-            live = (at >= 0) & (at < limit)
-            pl.when(live)(lambda: combine(way, source, lax.rem(at, chunks)))
-            return unused
-
-        lax.fori_loop(0, 6, combine_way, 0)
-        return unused
-
-    last = chunks * (steps - 1) + SERVE_LAG + COMBINE_LAG + chunks
-    lax.fori_loop(0, last, stage, 0)
 
     ahead = 2 * (2 * outer - (steps - 1))
     delays = (jnp.maximum(ahead, 0), jnp.maximum(-ahead, 0))
@@ -831,7 +771,90 @@
             pl.when(live)(add)
         return unused
 
-    lax.fori_loop(0, (steps - 1) * chunks + 2 * (steps - 1), pass_sums, 0)
+    edge = (outer == 0) | (outer == steps - 1)
+    serve_lag = jnp.where(edge, EDGE_SERVE_LAG, SERVE_LAG)
+    combine_lag = jnp.where(edge, EDGE_COMBINE_LAG, COMBINE_LAG)
+    for copy in loads[:3]:
+        copy.wait()
+
+    def first(chunk, unused):
+        dispatch(outer, chunk)
+        return unused
+
+    lax.fori_loop(0, chunks, first, 0)
+
+    def stage(number, unused):
+        def load_weights():
+            for copy in loads[3:]:
+                copy.wait()
+
+        def each_way(way, unused):
+            full = jnp.where(way == 0, depth[0], depth[1])
+
+            def take():
+                receive(way, number, full)
+
+                def rest():
+                    for part in order[2 + half :]:
+                        line_copy(way, 1, part, True).start()
+
+                pl.when((number == full * chunks - 1) & on_line(outer + 1 - 2 * way))(rest)
+                step, chunk, source = place_of(way, number, full)
+                dispatch(source, chunk)
+
+            pl.when(number < full * chunks)(take)
+            return unused
+
+        lax.fori_loop(0, 2, each_way, 0)
+        pl.when(number == 0)(load_weights)
+
+        def serve_way(way, unused):
+            full = jnp.where(way == 0, depth[0], depth[1])
+            at = number - serve_lag
+            step, chunk, source = place_of(way, at, full)
+            mine = way == 2
+            source = jnp.where(mine, outer, source)
+            chunk = jnp.where(mine, number, chunk)
+            live = jnp.where(mine, number < chunks, (at >= 0) & (at < full * chunks))
+            pl.when(live)(lambda: serve(source, chunk))
+            return unused
+
+        lax.fori_loop(0, 3, serve_way, 0)
+
+        def combine_way(turn, unused):
+            way = turn // 2
+            full = jnp.where(way == 0, depth[0], depth[1])
+            start = (full + 1) * half - 1 + serve_lag + combine_lag
+            raw = 2 * (number - start) + lax.rem(turn, 2)
+            later = raw - 2 * gap
+            mine = way == 2
+            at = jnp.where(raw < chunks, raw, later)
+            at = jnp.where(mine, 2 * (number - (chunks + combine_lag)) + lax.rem(turn, 2), at)
+            timely = mine | (raw < chunks) | (later >= chunks)
+            source = jnp.where(mine, outer, outer - (1 - 2 * way) * (full - at // chunks))
+            limit = jnp.where(mine, chunks, full * chunks)
+            live = timely & (at >= 0) & (at < limit)
+            pl.when(live)(lambda: combine(way, source, lax.rem(at, chunks)))
+            return unused
+
+        lax.fori_loop(0, 6, combine_way, 0)
+        deep = jnp.maximum(depth[0], depth[1])
+        opening = (deep + 1) * half - 1 + serve_lag + combine_lag + PASS_LAG
+
+        def pass_one(turn, unused):
+            def go():
+                pass_sums(2 * (number - opening) + turn, 0)
+
+            pl.when(number >= opening)(go)
+            return unused
+
+        lax.fori_loop(0, 2, pass_one, 0)
+        return unused
+
+    gap = jnp.where(edge, 0, PASS_GAP)
+    most = max(SERVE_LAG + COMBINE_LAG, EDGE_SERVE_LAG + EDGE_COMBINE_LAG)
+    last = chunks * (steps - 1) + most + chunks + PASS_LAG + half * (steps - 1)
+    lax.fori_loop(0, last, stage, 0)
 
     def gather(chunk):
         def from_way(way, unused):
@@ -922,6 +945,7 @@
             pltpu.VMEM((chunks, rows, width), f32),
             pltpu.VMEM((steps, spots, hidden), f32),
             pltpu.VMEM((steps, spots, hidden), f32),
+            pltpu.VMEM((steps, spots, rows), bf16),
             pltpu.VMEM((3, top, rows, spots), bf16),
             pltpu.VMEM((3, top, rows, HEAD), f32),
             pltpu.VMEM((chunks, width, hidden), gate.dtype),

time: 135 us -> 122 us (0.904)
  Pallas kernels: 130 us -> 120 us
  other arithmetic: 1.71 us -> 0.01 us
    pallas_call x1, Pallas kernels: 43.8 us -> 37.6 us  [run_front(): pl.pallas_call(functools.partial(front_kernel, size, pair, tp_size), out_...]
    pallas_call x1, Pallas kernels: 85.9 us -> 82 us  [run_experts(): pl.pallas_call(functools.partial(expert_kernel, steps, plane, tp_size), o...]
    broadcast_in_dim x3 -> x0, local copies, waits for them, and re-layouts: 1.52 us -> none  [the longest x1 1.52 us: run_front(): query_docs = jnp.broadcast_to(documents[:, None], (rows, HEAD))]
    another operation x4 -> x0, other arithmetic: 1.39 us -> none  [trig_tables(): jnp.stack([jnp.concatenate(order(cosine, cosine), axis=1), jnp.concatenat...]
where the time goes in v4:
time: 122 us
  Pallas kernels  120 us (98%)
  local copies, waits for them, and re-layouts  2.48 us (2%)
    pallas_call x1, Pallas kernels, run_experts(): pl.pallas_call(functools.partial(expert_kernel, steps, plane, tp_size), o...  82 us
    pallas_call x1, Pallas kernels, run_front(): pl.pallas_call(functools.partial(front_kernel, size, pair, tp_size), out_...  37.6 us

profile of v4, /device:TPU:9, one launch (start us, length us, event | category | flops | bytes accessed | tf_op | source)
XLA Modules:
  0.0 122.1 jit_solution(16307566983014630637)
XLA Ops:
  0.0 0.6 broadcast_in_dim_tile.3.freq_ref
  0.6 37.6 %shard_map.172.x_ref = bf16[4,128,512]{2,1,0:T(8,128)(2,1)} custom-call(bf16[512,256]{1,0:T(8,128)(2,1)} %q_ref.1, bf16[512,128]{1,0:T(8,128)(2,1)} %k_ref.1, bf16[512,128]{1,0:T(8,128)(2,1)} %v_ref.1, s32[4,128]{1,0:T(4,128)} %bitcast.21, f32[1,128]{1,0:T(1,128)} %bitcast.24, f32[1,128]{1,0:T(1,128)} %bitcast.25, f32[1,128]{1,0:T(1,128)} %broadcast_in_dim_tile.3.freq_ref, ...), custom_call_target="tpu_custom_call" | custom-call | tf_op jit(solution)/shard_map/pallas_call | solution.py:380
  38.2 82.0 %shard_map.173 = bf16[128,2048]{1,0:T(8,128)(2,1)} custom-call(bf16[4,128,512]{2,1,0:T(8,128)(2,1)} %shard_map.172.x_ref, s32[2,128]{1,0:T(2,128)} %bitcast.22, f32[2,128]{1,0:T(2,128)} %bitcast.23, bf16[4,512,512]{2,1,0:T(8,128)(2,1)} %bitcast.13, bf16[4,512,512]{2,1,0:T(8,128)(2,1)} %bitcast.14, bf16[512,2048]{1,0:T(8,128)(2,1)} %bitcast.15, ...), custom_call_target="tpu_custom_call" | custom-call | tf_op jit(solution)/shard_map/pallas_call | solution.py:929
  120.2 1.9 %copy.20 = bf16[128,2048]{1,0:T(8,128)(2,1)} copy(bf16[128,2048]{1,0:T(8,128)(2,1)} %shard_map.173) | data formatting | bytes 1048576
  (2 shorter events, 0.0 us)

commit v5 on v4

--- a/solution.py
+++ b/solution.py
@@ -2,6 +2,7 @@
 
 import jax
 import jax.numpy as jnp
+import numpy as np
 from jax import lax
 from jax.experimental import pallas as pl
 from jax.experimental.pallas import tpu as pltpu
@@ -9,11 +10,12 @@
 
 HEAD = 128
 GRID = 64
+LONGEST = (5, 8)
 CHUNKS = 4
-SERVE_LAG = 3
+SERVE_LAG = 4
 COMBINE_LAG = 2
 EDGE_SERVE_LAG = 2
-EDGE_COMBINE_LAG = 2
+EDGE_COMBINE_LAG = 1
 PASS_LAG = 2
 PASS_GAP = 2
 
@@ -84,7 +86,7 @@
     mate = outer * pair + lax.rem(inner + 1, pair)
     rows = k_ref.shape[0]
     pieces = doc_ref.shape[0]
-    grouped = q_rot.shape[0]
+    grouped = q_rot.shape[0] // rows
     parts = 3
 
     load = pltpu.make_async_copy(proj_hbm, proj, own_sem.at[0])
@@ -116,7 +118,6 @@
     tp_targets = [lax.rem(lane + step, tp_size) for step in range(1, tp_size)]
     for target in tp_targets:
         greet({"tp": target})
-    pl.semaphore_wait(barrier, peers)
 
     def piece(place, part, first):
         if part == 2:
@@ -157,8 +158,6 @@
         if pair == 2:
             mate_copy(0, 0, part, True).start()
 
-    send_own(1)
-    send_own(2)
     lanes = lax.broadcasted_iota(jnp.int32, (1, HEAD), 1)
     along = lax.rem(lanes, HEAD // 2) < HEAD // 4
     side = jnp.where(lanes < HEAD // 2, -1.0, 1.0)
@@ -183,13 +182,16 @@
         return unused
 
     lax.fori_loop(0, grid_rows, turn_keys, 0)
-    send_own(0)
+    pl.semaphore_wait(barrier, peers)
+    for part in (1, 2, 0):
+        send_own(part)
 
     def turn_queries(block, unused):
         cosine, sine = tables(block)
         here = pl.ds(pl.multiple_of(block * span, span), span)
         for head in range(grouped):
-            q_rot[head, here] = turned(
+            there = pl.ds(pl.multiple_of(head * rows + block * span, span), span)
+            q_rot[there] = turned(
                 q_ref[here, head * HEAD : (head + 1) * HEAD].astype(jnp.float32),
                 q_gain_ref[...],
                 cosine,
@@ -203,44 +205,37 @@
     for number in range(pieces):
         named = doc_ref[number : number + 1].astype(jnp.float32)
         column = jnp.sum(jnp.where(down == over, named, 0.0), axis=1, keepdims=True)
-        qdoc_ref[number * HEAD : (number + 1) * HEAD] = jnp.broadcast_to(
-            column, (HEAD, HEAD)
-        ).astype(jnp.int32)
+        column = jnp.broadcast_to(column, (HEAD, HEAD)).astype(jnp.int32)
+        for head in range(grouped):
+            qdoc_ref[pl.ds(head * rows + number * HEAD, HEAD)] = column
     m_ref[...] = jnp.full(m_ref.shape, -1e30, jnp.float32)
     l_ref[...] = jnp.zeros(l_ref.shape, jnp.float32)
     acc_ref[...] = jnp.zeros(acc_ref.shape, jnp.float32)
     for copy in own:
         copy.wait()
-    chunk = 256
 
     def advance(place):
         keys = kv[place, 0]
         values = kv[place, 1]
         doc_rows = docs[place]
         key_docs = jnp.concatenate([doc_rows[i : i + 1] for i in range(pieces)], axis=1)
-        for head in range(grouped):
-            for first in range(0, rows, chunk):
-                part = pl.ds(first, chunk)
-                scores = lax.dot_general(
-                    q_rot[head, part],
-                    keys,
-                    (((1,), (1,)), ((), ())),
-                    preferred_element_type=jnp.float32,
-                )
-                allowed = qdoc_ref[part, 0:1] == key_docs
-                scores = jnp.where(allowed, scores * score_factor, -1e30)
-                old_max = m_ref[head, part]
-                new_max = jnp.maximum(old_max, jnp.max(scores, axis=1, keepdims=True))
-                base = jnp.maximum(new_max[:, 0:1], -1e29)
-                weights = jnp.exp2(scores - base)
-                rescale = jnp.exp2(old_max - new_max)
-                l_ref[head, part] = l_ref[head, part] * rescale + jnp.sum(
-                    weights, axis=1, keepdims=True
-                )
-                acc_ref[head, part] = acc_ref[head, part] * rescale + jnp.dot(
-                    weights.astype(jnp.bfloat16), values, preferred_element_type=jnp.float32
-                )
-                m_ref[head, part] = new_max
+        scores = lax.dot_general(
+            q_rot[...], keys, (((1,), (1,)), ((), ())), preferred_element_type=jnp.float32
+        )
+        allowed = qdoc_ref[:, 0:1] == key_docs
+        scores = jnp.where(allowed, scores * score_factor, -1e30)
+        old_max = m_ref[...]
+        new_max = jnp.maximum(old_max, jnp.max(scores, axis=1, keepdims=True))
+        base = jnp.maximum(new_max[:, 0:1], -1e29)
+        weights = jnp.exp2(scores - base)
+        rescale = jnp.exp2(old_max - new_max)
+        l_ref[...] = l_ref[...] * rescale + jnp.sum(weights, axis=1, keepdims=True)
+        acc_ref[...] = acc_ref[...] * rescale + jnp.dot(
+            weights.astype(jnp.bfloat16), values, preferred_element_type=jnp.float32
+        )
+        m_ref[...] = new_max
+
+    reach = (size * rows * LONGEST[0] // LONGEST[1] - 2) // rows + 1
 
     def receive(step):
         for group in ((1, 2), (0,)):
@@ -276,7 +271,9 @@
                             mate_copy(way, step, part).wait_recv()
 
                     pl.when(across == 1)(arrive)
-                advance(there * pair + lax.rem(inner + across, pair))
+                block = there * pair + lax.rem(inner + across, pair)
+                close = (block - me <= reach) & (me - block <= reach)
+                pl.when(close)(lambda: advance(block))
 
             pl.when(on_line(there) & ((step > 0) | (way == 0)))(work)
             return unused
@@ -288,7 +285,9 @@
 
     lax.fori_loop(0, steps, stage, 0)
     for head in range(grouped):
-        o_buf[:, head * HEAD : (head + 1) * HEAD] = (acc_ref[head] / l_ref[head]).astype(
+        o_buf[:, head * HEAD : (head + 1) * HEAD] = (
+            acc_ref[head * rows : (head + 1) * rows] / l_ref[head * rows : (head + 1) * rows]
+        ).astype(
             o_buf.dtype
         )
 
@@ -375,7 +374,7 @@
     out_rows, model_width = residual.shape
     steps = size // pair
     pair_count = HEAD // 4
-    inv_freq = theta_base ** (-jnp.arange(pair_count, dtype=jnp.float32) / pair_count)
+    inv_freq = theta_base ** (-np.arange(pair_count, dtype=np.float32) / pair_count)
     dma = pltpu.SemaphoreType.DMA
     return pl.pallas_call(
         functools.partial(front_kernel, size, pair, tp_size),
@@ -385,13 +384,13 @@
         scratch_shapes=[
             pltpu.VMEM((size, 2, rows, HEAD), jnp.bfloat16),
             pltpu.VMEM((size, rows // HEAD, HEAD), jnp.int32),
-            pltpu.VMEM((rows, HEAD), jnp.int32),
+            pltpu.VMEM((grouped * rows, HEAD), jnp.int32),
             pltpu.VMEM((2, rows // GRID, HEAD), jnp.float32),
             pltpu.VMEM((2, GRID, HEAD), jnp.float32),
-            pltpu.VMEM((grouped, rows, HEAD), jnp.bfloat16),
-            pltpu.VMEM((grouped, rows, HEAD), jnp.float32),
-            pltpu.VMEM((grouped, rows, HEAD), jnp.float32),
-            pltpu.VMEM((grouped, rows, HEAD), jnp.float32),
+            pltpu.VMEM((grouped * rows, HEAD), jnp.bfloat16),
+            pltpu.VMEM((grouped * rows, HEAD), jnp.float32),
+            pltpu.VMEM((grouped * rows, HEAD), jnp.float32),
+            pltpu.VMEM((grouped * rows, HEAD), jnp.float32),
             pltpu.VMEM((rows, width), jnp.bfloat16),
             pltpu.VMEM((out_rows, width * tp_size), jnp.bfloat16),
             pltpu.VMEM(out_proj.shape, out_proj.dtype),
@@ -413,7 +412,7 @@
         documents.reshape(rows // HEAD, HEAD),
         query_gain[None, :],
         key_gain[None, :],
-        jnp.tile(inv_freq, 4)[None, :],
+        np.tile(inv_freq.astype(np.float32), 4)[None, :],
         out_gain[None, :],
         out_proj,
         residual,
@@ -513,7 +512,6 @@
         return unused
 
     lax.fori_loop(1, plane, greet_plane, 0)
-    pl.semaphore_wait(barrier, peers)
 
     def piece(place, part, first):
         if part == chunks:
@@ -542,10 +540,6 @@
         there = on_line(outer + 1 - 2 * way)
         for part in send:
             pl.when(there)(lambda part=part: line_copy(way, 1, part, True).start())
-
-    for way in range(2):
-        send_own(way, order[: 2 + half])
-        pl.when(depth[way] == 0)(lambda way=way: send_own(way, order[2 + half :]))
 
     def out_copy(source, chunk, target):
         return pltpu.make_async_remote_copy(
@@ -635,10 +629,15 @@
 
     def dispatch(source, chunk):
         pl.when(chunk == 0)(lambda: place_rows(source))
+        choose(source, chunk)
+        hand_out(source, chunk)
+
+    def choose(source, chunk):
         picked = jnp.dot(selects[source], xs[source, chunk], preferred_element_type=jnp.float32)
         outb[source, chunk] = picked.astype(jnp.bfloat16).reshape(plane, block, width)
         held[source, chunk, inner] = outb[source, chunk, inner]
 
+    def hand_out(source, chunk):
         def give(number, unused):
             out_copy(source, chunk, lax.rem(inner + number, plane)).start()
             return unused
@@ -774,14 +773,20 @@
     edge = (outer == 0) | (outer == steps - 1)
     serve_lag = jnp.where(edge, EDGE_SERVE_LAG, SERVE_LAG)
     combine_lag = jnp.where(edge, EDGE_COMBINE_LAG, COMBINE_LAG)
+    pl.semaphore_wait(barrier, peers)
+    for way in range(2):
+        send_own(way, order[: 2 + half])
+        pl.when(depth[way] == 0)(lambda way=way: send_own(way, order[2 + half :]))
     for copy in loads[:3]:
         copy.wait()
 
-    def first(chunk, unused):
-        dispatch(outer, chunk)
+    def own_rows(chunk, unused):
+        choose(outer, chunk)
+        hand_out(outer, chunk)
         return unused
 
-    lax.fori_loop(0, chunks, first, 0)
+    place_rows(outer)
+    lax.fori_loop(0, chunks, own_rows, 0)
 
     def stage(number, unused):
         def load_weights():

time: 122 us -> 119 us (0.975)
  Pallas kernels: 120 us -> 117 us
    pallas_call x1, Pallas kernels: 82 us -> 79.3 us  [run_experts(): pl.pallas_call(functools.partial(expert_kernel, steps, plane, tp_size), o...]
where the time goes in v5:
time: 119 us; the launch traced here: 118 us
  Pallas kernels  117 us (98%)
  local copies, waits for them, and re-layouts  1.88 us (2%)
    pallas_call x1, Pallas kernels, run_experts(): pl.pallas_call(functools.partial(expert_kernel, steps, plane, tp_size), o...  79.3 us
    pallas_call x1, Pallas kernels, run_front(): pl.pallas_call(functools.partial(front_kernel, size, pair, tp_size), out_...  37.3 us

profile of v5, /device:TPU:9, one launch (start us, length us, event | category | flops | bytes accessed | tf_op | source)
XLA Modules:
  0.0 118.5 jit_solution(17745487493072870600)
XLA Ops:
  0.0 37.3 %shard_map.181.x_ref = bf16[4,128,512]{2,1,0:T(8,128)(2,1)} custom-call(bf16[512,256]{1,0:T(8,128)(2,1)} %q_ref.1, bf16[512,128]{1,0:T(8,128)(2,1)} %k_ref.1, bf16[512,128]{1,0:T(8,128)(2,1)} %v_ref.1, s32[4,128]{1,0:T(4,128)} %bitcast.21, f32[1,128]{1,0:T(1,128)} %bitcast.24, f32[1,128]{1,0:T(1,128)} %bitcast.25, f32[1,128]{1,0:T(1,128)} %constant.2.clone.freq_ref, ...), custom_call_target="tpu_custom_call" | custom-call | tf_op jit(solution)/shard_map/pallas_call | solution.py:379
  37.3 79.3 %shard_map.182 = bf16[128,2048]{1,0:T(8,128)(2,1)} custom-call(bf16[4,128,512]{2,1,0:T(8,128)(2,1)} %shard_map.181.x_ref, s32[2,128]{1,0:T(2,128)} %bitcast.22, f32[2,128]{1,0:T(2,128)} %bitcast.23, bf16[4,512,512]{2,1,0:T(8,128)(2,1)} %bitcast.13, bf16[4,512,512]{2,1,0:T(8,128)(2,1)} %bitcast.14, bf16[512,2048]{1,0:T(8,128)(2,1)} %bitcast.15, ...), custom_call_target="tpu_custom_call" | custom-call | tf_op jit(solution)/shard_map/pallas_call | solution.py:934
  116.6 1.9 %copy.21 = bf16[128,2048]{1,0:T(8,128)(2,1)} copy(bf16[128,2048]{1,0:T(8,128)(2,1)} %shard_map.182) | data formatting | bytes 1048576

commit v6 on v5

--- a/solution.py
+++ b/solution.py
@@ -15,7 +15,7 @@
 SERVE_LAG = 4
 COMBINE_LAG = 2
 EDGE_SERVE_LAG = 2
-EDGE_COMBINE_LAG = 1
+EDGE_COMBINE_LAG = 0
 PASS_LAG = 2
 PASS_GAP = 2
 
@@ -378,7 +378,7 @@
     dma = pltpu.SemaphoreType.DMA
     return pl.pallas_call(
         functools.partial(front_kernel, size, pair, tp_size),
-        out_shape=jax.ShapeDtypeStruct((chunks, out_rows, model_width // chunks), jnp.bfloat16),
+        out_shape=pltpu.VMEM((chunks, out_rows, model_width // chunks), jnp.bfloat16),
         in_specs=[VMEM] * 8 + [ANY] + [VMEM] * 3,
         out_specs=VMEM,
         scratch_shapes=[

time: 119 us -> 118 us (level)
  Pallas kernels: 117 us -> 115 us
    unnamed x1 -> x3, local copies, waits for them, and re-layouts: 1.88 us -> 2.67 us
where the time goes in v6:
time: 118 us
  Pallas kernels  115 us (97%)
  local copies, waits for them, and re-layouts  2.67 us (2%)
    pallas_call x1, Pallas kernels, run_experts(): pl.pallas_call(functools.partial(expert_kernel, steps, plane, tp_size), o...  78.8 us
    pallas_call x1, Pallas kernels, run_front(): pl.pallas_call(functools.partial(front_kernel, size, pair, tp_size), out_...  36.6 us
    unnamed x3, local copies, waits for them, and re-layouts  2.67 us

profile of v6, /device:TPU:9, one launch (start us, length us, event | category | flops | bytes accessed | tf_op | source)
XLA Modules:
  0.0 118.1 jit_solution(3985235779503507809)
XLA Ops:
  0.0 36.6 %shard_map.181.x_ref = bf16[4,128,512]{2,1,0:T(8,128)(2,1)S(1)} custom-call(bf16[512,256]{1,0:T(8,128)(2,1)} %q_ref.1, bf16[512,128]{1,0:T(8,128)(2,1)} %k_ref.1, bf16[512,128]{1,0:T(8,128)(2,1)} %v_ref.1, s32[4,128]{1,0:T(4,128)} %bitcast.21, f32[1,128]{1,0:T(1,128)} %bitcast.24, f32[1,128]{1,0:T(1,128)} %bitcast.25, f32[1,128]{1,0:T(1,128)} %constant.2.clone.freq_ref, ...), custom_call_target="tpu_custom_call" | custom-call | tf_op jit(solution)/shard_map/pallas_call | solution.py:379
  36.6 0.0 copy-start
  36.6 0.8 copy-done
  37.4 78.8 %shard_map.182 = bf16[128,2048]{1,0:T(8,128)(2,1)} custom-call(bf16[4,128,512]{2,1,0:T(8,128)(2,1)} %copy-done, s32[2,128]{1,0:T(2,128)} %bitcast.22, f32[2,128]{1,0:T(2,128)} %bitcast.23, bf16[4,512,512]{2,1,0:T(8,128)(2,1)} %bitcast.13, bf16[4,512,512]{2,1,0:T(8,128)(2,1)} %bitcast.14, bf16[512,2048]{1,0:T(8,128)(2,1)} %bitcast.15, f32[1,2048]{1,0:T(1,128)} %bitcast.18, ...), custom_call_target="tpu_custom_call" | custom-call | tf_op jit(solution)/shard_map/pallas_call | solution.py:934
  116.2 1.9 %copy.21 = bf16[128,2048]{1,0:T(8,128)(2,1)} copy(bf16[128,2048]{1,0:T(8,128)(2,1)} %shard_map.182) | data formatting | bytes 1048576
Async XLA Ops:
  36.6 0.8 copy-start
